TPU v7x, 128 devices: a whole 4x4x4 slice. The times are simulated.
128 devices in a mesh: sp: 16 (over z, x), tp: 8 (over y, core).
Axes of the slice: x: 4, y: 4, z: 4, core: 2. Of those that a mesh axis runs over, the one named last changes fastest.
Arguments:
- tokens: bfloat16 [16384, 2048], P('sp', 'tp'), may hold values from -16 to 16
- norm_gain: float32 [2048], replicated, may hold values from 0.1 to 1.9
- signal_proj: bfloat16 [2048, 1024], P(None, 'tp'), may hold values from -0.125 to 0.125
- postgate_proj: bfloat16 [2048, 1024], P(None, 'tp'), may hold values from -0.125 to 0.125
- pregate_proj: bfloat16 [2048, 1024], P(None, 'tp'), may hold values from -0.125 to 0.125
- query_proj: bfloat16 [2048, 1024], P(None, 'tp'), may hold values from -0.21875 to 0.21875
- key_proj: bfloat16 [2048, 1024], P(None, 'tp'), may hold values from -0.21875 to 0.21875
- value_proj: bfloat16 [2048, 1024], P(None, 'tp'), may hold values from -0.125 to 0.125
- filter_taps: bfloat16 [3, 1024], P(None, 'tp'), may hold values from -3.5 to 3.5
- break_bias: bfloat16 [16384, 16], P('sp', 'tp'), may hold values from -18 to 0
- filter_readout: bfloat16 [1024, 2048], replicated, may hold values from -0.125 to 0.125
- attention_readout: bfloat16 [1024, 2048], replicated, may hold values from -0.125 to 0.125
Outputs:
- mixed: bfloat16 [16384, 2048], P(('sp', 'tp'))
- mass_logarithm: float32 [16, 16384], P('tp', 'sp')
All inputs are finite; a program needn't handle non-finite values.
Results may differ from a plain program's by a relative error of at most 0.013.
Values may be sent and summed in bfloat16 or wider, within the bound.
A program may use at most 128 MiB of HBM per device.

v0:
```python
import jax
import jax.numpy as jnp
from jax import lax
from jax.sharding import PartitionSpec as P

HEAD_DIM = 64
CONV_W = 3


epsilon = 1e-06
mass_floor = 0.1


def passed_along(block, axis, distance):
    devices = range(lax.axis_size(axis))
    route = [(i - distance, i) for i in devices if i - distance in devices]
    return lax.ppermute(block, axis, route)


def side_by_side(arrays, axis, dim, along):
    both = jnp.concatenate(arrays, axis=along)
    whole, at, finished = (lax.all_gather(both, axis, axis=dim, tiled=True), 0, [])
    for a in arrays:
        finished.append(lax.slice_in_dim(whole, at, at + a.shape[along], axis=along))
        at += a.shape[along]
    return tuple(finished)


def swapped(shard, axis, apart):
    return lax.ppermute(shard, axis, [(i, i ^ 1 << apart) for i in range(lax.axis_size(axis))])


def block_terms(queries3, key_rows, value_rows, bias_rows, own_block, row_offset):
    heads_dev = bias_rows.shape[1]
    key_heads = key_rows.reshape(key_rows.shape[0], heads_dev, HEAD_DIM)
    value_heads = value_rows.reshape(value_rows.shape[0], heads_dev, HEAD_DIM)
    scores = jnp.einsum("thd,shd->hts", queries3, key_heads, preferred_element_type=jnp.float32)
    scores = scores * HEAD_DIM ** (-0.5) + bias_rows.astype(jnp.float32).T[:, None, :]
    log_remainder = jax.nn.log_sigmoid(-scores)
    if own_block:
        row_ids = lax.broadcasted_iota(jnp.int32, scores.shape[1:], 0) + row_offset
        col_ids = lax.broadcasted_iota(jnp.int32, scores.shape[1:], 1)
        allowed = (col_ids < row_ids)[None]
        log_remainder = jnp.where(allowed, log_remainder, 0.0)
    running = jnp.cumsum(log_remainder, axis=2)
    block_total = running[:, :, -1:]
    weights = jnp.exp(jax.nn.log_sigmoid(scores) + (block_total - running))
    if own_block:
        weights = jnp.where(allowed, weights, 0.0)
    partial_value = jnp.einsum(
        "hts,shd->thd",
        weights.astype(jnp.bfloat16),
        value_heads,
        preferred_element_type=jnp.float32,
    )
    return (partial_value, block_total[:, :, 0])


def per_device(
    tokens,
    norm_gain,
    signal_proj,
    postgate_proj,
    pregate_proj,
    query_proj,
    key_proj,
    value_proj,
    filter_taps,
    break_bias,
    filter_readout,
    attention_readout,
):
    tok_dev = tokens.shape[0]
    heads_dev = break_bias.shape[1]
    projections = (signal_proj, postgate_proj, pregate_proj, query_proj, key_proj, value_proj)
    whole_rows = lax.all_gather(tokens, "tp", axis=1, tiled=True)
    widened = whole_rows.astype(jnp.float32)
    inverse = lax.rsqrt(jnp.mean(widened * widened, axis=1) + epsilon)
    scaled = (widened * norm_gain[None, :]).astype(jnp.bfloat16)
    products = tuple(
        (jnp.dot(scaled, weight, preferred_element_type=jnp.float32) for weight in projections)
    )
    signal, post_gate, pre_gate, queries, key_rows, value_rows = tuple(
        ((product * inverse[:, None]).astype(jnp.bfloat16) for product in products)
    )
    rim_width = CONV_W - 1
    rim_signal, rim_pre = passed_along(
        (signal[tok_dev - rim_width :], pre_gate[tok_dev - rim_width :]), "sp", 1
    )
    extended = jnp.concatenate(
        [
            rim_pre.astype(jnp.float32) * rim_signal.astype(jnp.float32),
            pre_gate.astype(jnp.float32) * signal.astype(jnp.float32),
        ],
        axis=0,
    )
    tap_values = filter_taps.astype(jnp.float32)
    running = jnp.zeros((tok_dev, extended.shape[1]), jnp.float32)
    for offset in range(CONV_W):
        running = running + tap_values[offset][None, :] * extended[offset : offset + tok_dev]
    filtered = (post_gate.astype(jnp.float32) * running).astype(jnp.bfloat16)
    queries3 = queries.reshape(tok_dev, heads_dev, HEAD_DIM)
    position = lax.axis_index("sp")
    all_keys, all_values, all_bias = side_by_side((key_rows, value_rows, break_bias), "sp", 0, 1)
    half_rows = tok_dev // 2
    seq_devices = lax.axis_size("sp")
    bit_count = seq_devices.bit_length() - 1
    mirror_queries = queries3[half_rows:]
    for bit in range(bit_count):
        mirror_queries = swapped(mirror_queries, "sp", bit)
    mirror_block = seq_devices - 1 - position

    def attend_rows(query_rows, block_index, row_offset):
        start = block_index * tok_dev
        first_out, first_remain = block_terms(
            query_rows,
            lax.dynamic_slice_in_dim(all_keys, start, tok_dev, 0),
            lax.dynamic_slice_in_dim(all_values, start, tok_dev, 0),
            lax.dynamic_slice_in_dim(all_bias, start, tok_dev, 0),
            True,
            row_offset,
        )

        def advance(distance, state):
            acc_out, acc_remain = state
            source = (block_index - distance) * tok_dev
            partial_value, remain = block_terms(
                query_rows,
                lax.dynamic_slice_in_dim(all_keys, source, tok_dev, 0),
                lax.dynamic_slice_in_dim(all_values, source, tok_dev, 0),
                lax.dynamic_slice_in_dim(all_bias, source, tok_dev, 0),
                False,
                0,
            )
            acc_out = acc_out + jnp.exp(acc_remain).T[:, :, None] * partial_value
            return (acc_out, acc_remain + remain)

        return lax.fori_loop(1, block_index + 1, advance, (first_out, first_remain))

    lower_out, lower_remain = attend_rows(queries3[:half_rows], position, 0)
    upper_out, upper_remain = attend_rows(mirror_queries, mirror_block, half_rows)
    for bit in range(bit_count):
        upper_out, upper_remain = (
            swapped(upper_out.astype(jnp.bfloat16), "sp", bit).astype(upper_out.dtype),
            swapped(upper_remain.astype(jnp.bfloat16), "sp", bit).astype(upper_remain.dtype),
        )
    acc_out = jnp.concatenate([lower_out, upper_out], axis=0)
    acc_remain = jnp.concatenate([lower_remain, upper_remain], axis=1)
    attended = acc_out.reshape(tok_dev, heads_dev * HEAD_DIM).astype(jnp.bfloat16)
    mass_logarithm = jnp.log(jnp.maximum(-jnp.expm1(acc_remain), mass_floor))
    filter_rows, attended_rows = (
        lax.all_to_all(filtered, "tp", split_axis=0, concat_axis=1, tiled=True),
        lax.all_to_all(attended, "tp", split_axis=0, concat_axis=1, tiled=True),
    )
    mixed = (
        jnp.dot(filter_rows, filter_readout, preferred_element_type=jnp.float32)
        + jnp.dot(attended_rows, attention_readout, preferred_element_type=jnp.float32)
    ).astype(jnp.bfloat16)
    return (mixed, mass_logarithm)


def solution(mesh):
    placed = (
        P("sp", "tp"),
        P(),
        P(None, "tp"),
        P(None, "tp"),
        P(None, "tp"),
        P(None, "tp"),
        P(None, "tp"),
        P(None, "tp"),
        P(None, "tp"),
        P("sp", "tp"),
        P(),
        P(),
    )
    return jax.shard_map(
        per_device,
        mesh=mesh,
        in_specs=placed,
        out_specs=(P(("sp", "tp"), None), P("tp", "sp")),
        check_vma=False,
    )
```

profile of v0, /device:TPU:38, one launch (start us, length us, event | category | flops | bytes accessed | tf_op | source)
XLA Modules:
  0.0 866.8 jit_solution(7214681377408366476)
XLA Ops:
  8.9 38.3 %all-gather.3.cloned.1.call-done = bf16[1024,2048]{1,0:T(8,128)(2,1)} async-done(((bf16[1024,256]{1,0:T(8,128)(2,1)}), bf16[1024,2048]{1,0:T(8,128)(2,1)}) %all-gather.3.cloned.1.call-update) | async-done | bytes 4194320 | tf_op jit(solution)/shard_map/all_gather | solution.py:76
  54.8 3.6 fusion.113
  63.9 4.7 convert_multiply_fusion.2
  68.6 4.3 collective-permute-start.1
  74.3 9.0 %collective-permute-done.3 = bf16[512,2,64]{0,2,1:T(8,128)(2,1)S(1)} collective-permute-done((bf16[512,2,64]{0,2,1:T(8,128)(2,1)S(1)}, bf16[512,2,64]{0,2,1:T(8,128)(2,1)S(1)}, u32[]{:S(2)}, u32[]{:S(2)}) %collective-permute-start.3) | collective-permute-done | bytes 131104 | tf_op jit(solution)/shard_map/ppermute | solution.py:30
  83.7 3.9 fusion.125
  88.5 4.1 all-to-all-start
  95.4 53.7 %all-gather.5.cloned.1.call-done = bf16[16384,258]{1,0:T(8,128)(2,1)} async-done(((bf16[1024,258]{1,0:T(8,128)(2,1)}), bf16[16384,258]{1,0:T(8,128)(2,1)}) %all-gather.5.cloned.1.call-update) | async-done | bytes 8454160 | tf_op jit(solution)/shard_map/all_gather | solution.py:22
  149.0 3.7 slice.111
  152.8 3.7 copy.117
  158.0 5.8 fusion.146
  163.8 6.4 copy.115
  170.2 6.5 copy.116
  178.4 5.1 fusion.65
  186.5 5.6 copy.122
  196.6 4.6 broadcast_add_fusion.2
  201.2 5.5 copy.123
  206.7 4.9 reduce_window_sum.49
  213.0 6.1 fusion.131
  219.1 153.0 %while.25 = (s32[]{:T(128)}, f32[512,2,64]{0,2,1:T(8,128)S(1)}, f32[2,512]{1,0:T(2,128)S(1)}, s32[]{:T(128)}, s32[]{:T(128)}, /*index=5*/bf16[16384,128]{0,1:T(8...) while((s32[]{:T(128)}, f32[512,2,64]{0,2,1:T(8,128)S(1)}, ...), condition=%wide.region_12.13_spmd, body=%wide.region_9.12_spmd.sunk | while | flops 425920512 | bytes 78029064 | solution.py:138
  220.4 4.4 fusion.207
  234.6 3.8 fusion.210
  239.5 4.4 fusion.207
  253.7 3.8 fusion.210
  258.6 4.4 fusion.207
  272.8 3.8 fusion.210
  277.7 4.4 fusion.207
  291.9 3.8 fusion.210
  296.8 4.4 fusion.207
  311.0 3.8 fusion.210
  315.9 4.4 fusion.207
  330.1 3.8 fusion.210
  335.0 4.4 fusion.207
  349.2 3.8 fusion.210
  354.1 4.4 fusion.207
  368.3 3.8 fusion.210
  372.1 20.1 %collective-permute-start.10 = (bf16[2,512]{1,0:T(2,128)(2,1)S(1)}, bf16[2,512]{1,0:T(2,128)(2,1)S(1)}, u32[]{:S(2)}, u32[]{:S(2)}) collective-permute-start(bf16[2,512]{1,0:T(2,128)(2,1)S(1)} %convert_element_type.111), channel_id=1, source_target_pairs={{0,8},{8,0},{16,24},{24,16},{32,40},{40,32},{48,56},{56,48},{64,72... | collective-permute-start | bytes 6152 | tf_op jit(solution)/shard_map/ppermute | solution.py:30
  392.6 5.1 fusion.58
  400.6 5.6 copy.113
  410.7 4.6 broadcast_add_fusion.3
  415.3 5.5 copy.114
  420.9 4.9 reduce_window_sum.47
  425.8 39.3 %collective-permute-start.7 = (bf16[512,2,64]{0,2,1:T(8,128)(2,1)S(1)}, bf16[512,2,64]{0,2,1:T(8,128)(2,1)S(1)}, u32[]{:S(2)}, u32[]{:S(2)}) collective-permute-start(bf16[512,2,64]{0,2,1:T(8,128)(2,1)S(1)} %collective-permute-done.6), channel_id=1, source_target_pairs={{0,16},{8,24},{16,0},{24,8},{32,48},{40,56},{48,32},{56,40},{64,80... | collective-permute-start | bytes 393224 | tf_op jit(solution)/shard_map/ppermute | solution.py:30
  468.2 78.2 %collective-permute-start.8 = (bf16[512,2,64]{0,2,1:T(8,128)(2,1)S(1)}, bf16[512,2,64]{0,2,1:T(8,128)(2,1)S(1)}, u32[]{:S(2)}, u32[]{:S(2)}) collective-permute-start(bf16[512,2,64]{0,2,1:T(8,128)(2,1)S(1)} %collective-permute-done.7), channel_id=1, source_target_pairs={{0,32},{8,40},{16,48},{24,56},{32,0},{40,8},{48,16},{56,24},{64,96... | collective-permute-start | bytes 393224 | tf_op jit(solution)/shard_map/ppermute | solution.py:30
  546.3 6.1 fusion.128
  552.7 134.0 %while.24 = (s32[]{:T(128)}, f32[512,2,64]{0,2,1:T(8,128)S(1)}, f32[2,512]{1,0:T(2,128)S(1)}, s32[]{:T(128)}, s32[]{:T(128)}, /*index=5*/bf16[16384,128]{0,1:T(8...) while((s32[]{:T(128)}, f32[512,2,64]{0,2,1:T(8,128)S(1)}, ...), condition=%wide.region_6.7_spmd, body=%wide.region_3.6_spmd.sunk | while | flops 425920512 | bytes 78029064 | solution.py:138
  554.0 4.4 fusion.198
  568.2 3.8 fusion.201
  573.1 4.4 fusion.198
  587.3 3.8 fusion.201
  592.2 4.4 fusion.198
  606.4 3.8 fusion.201
  611.3 4.4 fusion.198
  625.5 3.8 fusion.201
  630.4 4.4 fusion.198
  644.6 3.8 fusion.201
  649.5 4.4 fusion.198
  663.7 3.8 fusion.201
  668.6 4.4 fusion.198
  682.8 3.8 fusion.201
  686.7 156.4 %collective-permute-start.13 = (bf16[2,512]{1,0:T(2,128)(2,1)S(1)}, bf16[2,512]{1,0:T(2,128)(2,1)S(1)}, u32[]{:S(2)}, u32[]{:S(2)}) collective-permute-start(bf16[2,512]{1,0:T(2,128)(2,1)S(1)} %collective-permute-done.12), channel_id=1, source_target_pairs={{0,64},{8,72},{16,80},{24,88},{32,96},{40,104},{48,112},{56,120},{... | collective-permute-start | bytes 6152 | tf_op jit(solution)/shard_map/ppermute | solution.py:30
  843.9 4.5 all-to-all-start.1
  852.1 3.8 all-to-all-done.1
  855.8 3.7 fusion.66
  (326 shorter events, 209.9 us)
Async XLA Ops:
  7.2 56.8 %copy-start = (bf16[2048,128]{1,0:T(8,128)(2,1)S(1)}, bf16[2048,128]{1,0:T(8,128)(2,1)}, u32[]{:S(2)}) copy-start(bf16[2048,128]{1,0:T(8,128)(2,1)} %param.18) | copy-start | bytes 1572868
  7.2 43.3 %copy-start.14 = (f32[2048]{0:T(1024)S(1)}, f32[2048]{0:T(1024)}, u32[]{:S(2)}) copy-start(f32[2048]{0:T(1024)} %param.17) | copy-start | bytes 24580
  7.2 43.3 %copy-start.9 = (bf16[2048,128]{1,0:T(8,128)(2,1)S(1)}, bf16[2048,128]{1,0:T(8,128)(2,1)}, u32[]{:S(2)}) copy-start(bf16[2048,128]{1,0:T(8,128)(2,1)} %param.22) | copy-start | bytes 1572868
  7.2 40.0 %all-gather.3.cloned.1.call-start = ((), (), s32[]{:S(2)}) async-start(), calls=%async_computation.2 | async-start | bytes 4718592 | tf_op jit(solution)/shard_map/all_gather | solution.py:76
  7.9 141.1 %all-gather.5.cloned.1.call-start = ((), (), s32[]{:S(2)}) async-start(), calls=%async_computation.3 | async-start | bytes 13369344 | tf_op jit(solution)/shard_map/all_gather | solution.py:22
  47.2 3.4 copy-start.6
  50.6 1.3 copy-start.10
  51.9 2.3 copy-start.8
  51.9 2.9 copy-start.11
  54.8 7.1 copy-start.7
  54.8 7.1 copy-start.12
  58.5 15.8 %collective-permute-start = (bf16[2,128]{1,0:T(2,128)(2,1)S(1)}, bf16[2,128]{1,0:T(2,128)(2,1)S(1)}, u32[]{:S(2)}, u32[]{:S(2)}) collective-permute-start(bf16[2,128]{1,0:T(2,128)(2,1)S(1)} %slice.104), channel_id=1, source_target_pairs={{0,8},{8,16},{16,24},{24,32},{32,40},{40,48},{48,56},{56,64},{64,7... | collective-permute-start | bytes 1544 | tf_op jit(solution)/shard_map/ppermute | solution.py:17
  63.4 20.4 %copy-start.13 = (bf16[2048,128]{1,0:T(8,128)(2,1)S(1)}, bf16[2048,128]{1,0:T(8,128)(2,1)}, u32[]{:S(2)}) copy-start(bf16[2048,128]{1,0:T(8,128)(2,1)} %param.19) | copy-start | bytes 1572868
  63.4 9.6 %collective-permute-start.2 = (bf16[512,2,64]{0,2,1:T(8,128)(2,1)S(1)}, bf16[512,2,64]{0,2,1:T(8,128)(2,1)S(1)}, u32[]{:S(2)}, u32[]{:S(2)}) collective-permute-start(bf16[512,2,64]{0,2,1:T(8,128)(2,1)S(1)} %bitcast.246), channel_id=1, source_target_pairs={{0,8},{8,0},{16,24},{24,16},{32,40},{40,32},{48,56},{56,48},{64,72... | collective-permute-start | bytes 393224 | tf_op jit(solution)/shard_map/ppermute | solution.py:30
  68.6 5.7 collective-permute-start.1
  73.0 10.3 %collective-permute-start.3 = (bf16[512,2,64]{0,2,1:T(8,128)(2,1)S(1)}, bf16[512,2,64]{0,2,1:T(8,128)(2,1)S(1)}, u32[]{:S(2)}, u32[]{:S(2)}) collective-permute-start(bf16[512,2,64]{0,2,1:T(8,128)(2,1)S(1)} %collective-permute-done.2), channel_id=1, source_target_pairs={{0,16},{8,24},{16,0},{24,8},{32,48},{40,56},{48,32},{56,40},{64,80... | collective-permute-start | bytes 393224 | tf_op jit(solution)/shard_map/ppermute | solution.py:30
  83.3 9.3 %collective-permute-start.4 = (bf16[512,2,64]{0,2,1:T(8,128)(2,1)S(1)}, bf16[512,2,64]{0,2,1:T(8,128)(2,1)S(1)}, u32[]{:S(2)}, u32[]{:S(2)}) collective-permute-start(bf16[512,2,64]{0,2,1:T(8,128)(2,1)S(1)} %collective-permute-done.3), channel_id=1, source_target_pairs={{0,32},{8,40},{16,48},{24,56},{32,0},{40,8},{48,16},{56,24},{64,96... | collective-permute-start | bytes 393224 | tf_op jit(solution)/shard_map/ppermute | solution.py:30
  88.5 755.4 %all-to-all-start = ((bf16[8,128,128]{1,2,0:T(8,128)(2,1)}), bf16[8,128,128]{1,2,0:T(8,128)(2,1)}, u32[]{:S(2)}, u32[]{:S(2)}) async-start(bf16[8,128,128]{1,2,0:T(8,128)(2,1)} %copy.104), calls=%async_computation | async-start | bytes 524288 | tf_op jit(solution)/shard_map/all_to_all | solution.py:152
  92.6 85.9 %collective-permute-start.5 = (bf16[512,2,64]{0,2,1:T(8,128)(2,1)S(1)}, bf16[512,2,64]{0,2,1:T(8,128)(2,1)S(1)}, u32[]{:S(2)}, u32[]{:S(2)}) collective-permute-start(bf16[512,2,64]{0,2,1:T(8,128)(2,1)S(1)} %collective-permute-done.4), channel_id=1, source_target_pairs={{0,64},{8,72},{16,80},{24,88},{32,96},{40,104},{48,112},{56,120},{... | collective-permute-start | bytes 393224 | tf_op jit(solution)/shard_map/ppermute | solution.py:30
  194.5 1.9 copy-start.4
  227.4 1.9 copy-start.2
  232.1 2.5 copy-start.15
  246.5 1.9 copy-start.2
  251.2 2.5 copy-start.15
  265.6 1.9 copy-start.2
  270.3 2.5 copy-start.15
  284.7 1.9 copy-start.2
  289.4 2.5 copy-start.15
  303.8 1.9 copy-start.2
  308.5 2.5 copy-start.15
  322.9 1.9 copy-start.2
  327.6 2.5 copy-start.15
  342.0 1.9 copy-start.2
  346.7 2.5 copy-start.15
  361.1 1.9 copy-start.2
  365.8 2.5 copy-start.15
  372.1 94.5 %collective-permute-start.10 = (bf16[2,512]{1,0:T(2,128)(2,1)S(1)}, bf16[2,512]{1,0:T(2,128)(2,1)S(1)}, u32[]{:S(2)}, u32[]{:S(2)}) collective-permute-start(bf16[2,512]{1,0:T(2,128)(2,1)S(1)} %convert_element_type.111), channel_id=1, source_target_pairs={{0,8},{8,0},{16,24},{24,16},{32,40},{40,32},{48,56},{56,48},{64,72... | collective-permute-start | bytes 6152 | tf_op jit(solution)/shard_map/ppermute | solution.py:30
  392.3 33.5 %collective-permute-start.6 = (bf16[512,2,64]{0,2,1:T(8,128)(2,1)S(1)}, bf16[512,2,64]{0,2,1:T(8,128)(2,1)S(1)}, u32[]{:S(2)}, u32[]{:S(2)}) collective-permute-start(bf16[512,2,64]{0,2,1:T(8,128)(2,1)S(1)} %convert_element_type.108), channel_id=1, source_target_pairs={{0,8},{8,0},{16,24},{24,16},{32,40},{40,32},{48,56},{56,48},{64,72... | collective-permute-start | bytes 393224 | tf_op jit(solution)/shard_map/ppermute | solution.py:30
  408.7 1.9 copy-start.5
  425.8 42.4 %collective-permute-start.7 = (bf16[512,2,64]{0,2,1:T(8,128)(2,1)S(1)}, bf16[512,2,64]{0,2,1:T(8,128)(2,1)S(1)}, u32[]{:S(2)}, u32[]{:S(2)}) collective-permute-start(bf16[512,2,64]{0,2,1:T(8,128)(2,1)S(1)} %collective-permute-done.6), channel_id=1, source_target_pairs={{0,16},{8,24},{16,0},{24,8},{32,48},{40,56},{48,32},{56,40},{64,80... | collective-permute-start | bytes 393224 | tf_op jit(solution)/shard_map/ppermute | solution.py:30
  466.6 85.9 %collective-permute-start.11 = (bf16[2,512]{1,0:T(2,128)(2,1)S(1)}, bf16[2,512]{1,0:T(2,128)(2,1)S(1)}, u32[]{:S(2)}, u32[]{:S(2)}) collective-permute-start(bf16[2,512]{1,0:T(2,128)(2,1)S(1)} %collective-permute-done.10), channel_id=1, source_target_pairs={{0,16},{8,24},{16,0},{24,8},{32,48},{40,56},{48,32},{56,40},{64,80... | collective-permute-start | bytes 6152 | tf_op jit(solution)/shard_map/ppermute | solution.py:30
  468.2 84.4 %collective-permute-start.8 = (bf16[512,2,64]{0,2,1:T(8,128)(2,1)S(1)}, bf16[512,2,64]{0,2,1:T(8,128)(2,1)S(1)}, u32[]{:S(2)}, u32[]{:S(2)}) collective-permute-start(bf16[512,2,64]{0,2,1:T(8,128)(2,1)S(1)} %collective-permute-done.7), channel_id=1, source_target_pairs={{0,32},{8,40},{16,48},{24,56},{32,0},{40,8},{48,16},{56,24},{64,96... | collective-permute-start | bytes 393224 | tf_op jit(solution)/shard_map/ppermute | solution.py:30
  552.5 134.2 %collective-permute-start.12 = (bf16[2,512]{1,0:T(2,128)(2,1)S(1)}, bf16[2,512]{1,0:T(2,128)(2,1)S(1)}, u32[]{:S(2)}, u32[]{:S(2)}) collective-permute-start(bf16[2,512]{1,0:T(2,128)(2,1)S(1)} %collective-permute-done.11), channel_id=1, source_target_pairs={{0,32},{8,40},{16,48},{24,56},{32,0},{40,8},{48,16},{56,24},{64,96... | collective-permute-start | bytes 6152 | tf_op jit(solution)/shard_map/ppermute | solution.py:30
  552.6 290.4 %collective-permute-start.9 = (bf16[512,2,64]{0,2,1:T(8,128)(2,1)S(1)}, bf16[512,2,64]{0,2,1:T(8,128)(2,1)S(1)}, u32[]{:S(2)}, u32[]{:S(2)}) collective-permute-start(bf16[512,2,64]{0,2,1:T(8,128)(2,1)S(1)} %collective-permute-done.8), channel_id=1, source_target_pairs={{0,64},{8,72},{16,80},{24,88},{32,96},{40,104},{48,112},{56,120},{... | collective-permute-start | bytes 393224 | tf_op jit(solution)/shard_map/ppermute | solution.py:30
  561.0 1.9 copy-start.3
  565.7 2.5 copy-start.16
  580.1 1.9 copy-start.3
  584.8 2.5 copy-start.16
  599.2 1.9 copy-start.3
  603.9 2.5 copy-start.16
  618.3 1.9 copy-start.3
  623.0 2.5 copy-start.16
  637.4 1.9 copy-start.3
  642.1 2.5 copy-start.16
  656.5 1.9 copy-start.3
  661.2 2.5 copy-start.16
  675.6 1.9 copy-start.3
  680.3 2.5 copy-start.16
  686.7 164.7 %collective-permute-start.13 = (bf16[2,512]{1,0:T(2,128)(2,1)S(1)}, bf16[2,512]{1,0:T(2,128)(2,1)S(1)}, u32[]{:S(2)}, u32[]{:S(2)}) collective-permute-start(bf16[2,512]{1,0:T(2,128)(2,1)S(1)} %collective-permute-done.12), channel_id=1, source_target_pairs={{0,64},{8,72},{16,80},{24,88},{32,96},{40,104},{48,112},{56,120},{... | collective-permute-start | bytes 6152 | tf_op jit(solution)/shard_map/ppermute | solution.py:30
  843.9 12.0 %all-to-all-start.1 = ((bf16[8,128,128]{1,2,0:T(8,128)(2,1)}), bf16[8,128,128]{1,2,0:T(8,128)(2,1)S(1)}, u32[]{:S(2)}, u32[]{:S(2)}) async-start(bf16[8,128,128]{1,2,0:T(8,128)(2,1)} %copy.127), calls=%async_computation.1 | async-start | bytes 524288 | tf_op jit(solution)/shard_map/all_to_all | solution.py:153
  848.3 11.2 %copy-start.1 = (bf16[2048,128]{1,0:T(8,128)(2,1)S(1)}, bf16[2048,128]{1,0:T(8,128)(2,1)}, u32[]{:S(2)}) copy-start(bf16[2048,128]{1,0:T(8,128)(2,1)} %param.18) | copy-start | bytes 1572868
Sparse Core Ops, SparseCore 0:
  9.7 37.4 all-gather.2
  54.4 94.6 all-gather.4
where the time goes:
time: 877 us; the launch traced here: 867 us
  starting transfers between devices  316 us (36%)
  matrix products  168 us (19%)
  local copies, waits for them, and re-layouts  158 us (18%)
  waiting for transfers between devices  107 us (12%)
  other arithmetic  101 us (12%)
  between operations  15 us (2%)
    ppermute x12, starting transfers between devices, swapped(): lax.ppermute(shard, axis, [(i, i ^ 1 << apart) for i in range(lax.axis_si...  300 us
    another operation x52, other arithmetic  94.2 us
    dot_general x17, matrix products, block_terms(): jnp.einsum('thd,shd->hts', queries3, key_heads, preferred_element_type=jn...  75.7 us
    dot_general x17, matrix products, block_terms(): jnp.einsum('hts,shd->thd', weights.astype(jnp.bfloat16), value_heads, pre...  69.3 us
    another operation x55, local copies, waits for them, and re-layouts  68.5 us
    all_gather x1, waiting for transfers between devices, side_by_side(): lax.all_gather(both, axis, axis=dim, tiled=True)  53.7 us
    all_gather x1, waiting for transfers between devices, per_device(): whole_rows = lax.all_gather(tokens, 'tp', axis=1, tiled=True)  38.3 us
    while x75, local copies, waits for them, and re-layouts  29.2 us
  transfers between devices with their start and end apart: 18, of which 5 were waited for; matrix products, arithmetic and copies ran while one was open for 44% of the time, Pallas kernels for 0%

commit v1 on v0

v1 whole, which is shorter than its diff:
```python
import jax
import jax.numpy as jnp
from jax import lax
from jax.experimental import pallas as pl
from jax.experimental.pallas import tpu as pltpu
from jax.sharding import PartitionSpec as P

HEAD_DIM = 64
CONV_W = 3
CH = 256
NT = 4
CAP = 24.0
LOG2E = 1.4426950408889634
epsilon = 1e-06
mass_floor = 0.1


def scan_chunk(y_ref, carry_ref, w_ref, masked):
    groups = CH // 8
    seg = CH // 8
    if masked:
        row = lax.broadcasted_iota(jnp.int32, (8, CH), 0) * seg
        col = lax.broadcasted_iota(jnp.int32, (8, CH), 1)
        diff = col - row
    r = jnp.ones((8, CH), jnp.float32)
    for g in reversed(range(groups // 4)):
        us, ds = [], []
        for k in range(4):
            j = 4 * g + k
            y = y_ref[j * 8:(j + 1) * 8, :]
            u = jnp.exp2(jnp.minimum(y, CAP))
            if masked:
                u = jnp.where(diff > j, u, 0.0)
            us.append(u)
            ds.append(1.0 + u)
        prod = (ds[0] * ds[1]) * (ds[2] * ds[3])
        r = r * (1.0 / prod)
        e = r
        for k in range(4):
            j = 4 * g + k
            y_ref[j * 8:(j + 1) * 8, :] = us[k] * e
            if k < 3:
                e = e * ds[k]
    sub = lax.broadcasted_iota(jnp.int32, (8, CH), 0)
    s = r
    for k in (1, 2, 4):
        s = s * jnp.where(sub < 8 - k, pltpu.roll(s, 8 - k, 0), 1.0)
    excl = jnp.where(sub < 7, pltpu.roll(s, 7, 0), 1.0)
    carry = carry_ref[...]
    c = excl * carry
    carry_ref[...] = carry * jnp.broadcast_to(s[0:1, :], (8, CH))
    w = y_ref[...].reshape(CH // 8, 8, CH) * c[None]
    w_ref[...] = w.reshape(CH, CH).astype(jnp.bfloat16)

def qk(k_ref, q_ref, tile):
    kk = k_ref
    return jnp.dot(jnp.concatenate([kk, kk], axis=1), q_ref[:, tile * CH:(tile + 1) * CH],
                   preferred_element_type=jnp.float32)

def attend_set(qt, blk, kchunk, vchunk, acc, carry, ya, yb, wa, wb):
    base = 4 * blk
    for t in range(NT):
        acc[t] = jnp.zeros_like(acc[t])
        carry[t] = jnp.ones((8, CH), jnp.float32)
    for c in reversed(range(NT)):
        kk = kchunk(base + c)
        for t in range(c, NT):
            ya[t] = qk(kk, qt, t)
        for t in range(c, NT):
            scan_chunk(ya.at[t], carry.at[t], wb.at[t], t == c)
        if c > 0:
            vv = vchunk(base + c)
            for t in range(c, NT):
                acc[t] += jnp.dot(vv, wb[t], preferred_element_type=jnp.float32)
    kk = kchunk(jnp.maximum(base - 1, 0))
    for t in range(NT):
        ya[t] = qk(kk, qt, t)

    def half(c, ysrc, ydst, wdst, wsrc):
        kn = kchunk(jnp.maximum(c - 1, 0))
        vp = vchunk(c + 1)
        for t in range(NT):
            scan_chunk(ysrc.at[t], carry.at[t], wdst.at[t], False)
            ydst[t] = qk(kn, qt, t)
            acc[t] += jnp.dot(vp, wsrc[t], preferred_element_type=jnp.float32)

    def body(p, _):
        c = base - 1 - 2 * p
        half(c, ya, yb, wa, wb)
        half(c - 1, yb, ya, wb, wa)
        return 0
    lax.fori_loop(0, 2 * blk, body, 0)
    vp = vchunk(0)
    for t in range(NT):
        acc[t] += jnp.dot(vp, wb[t], preferred_element_type=jnp.float32)


def attention_kernel(qt, kp, vt, out, rem, acc, carry, ya, yb, wa, wb):
    me = lax.axis_index("sp")
    head = me // 8

    def kchunk(c):
        return kp[c // NT, head, pl.ds(pl.multiple_of((c % NT) * CH, CH), CH), :]

    def vchunk(c):
        return vt[c // NT, head, c % NT]

    for which in range(2):
        block = me if which == 0 else 15 - me
        attend_set(qt.at[which], block, kchunk, vchunk, acc, carry, ya, yb, wa, wb)
        for t in range(NT):
            out[which, :, t * CH:(t + 1) * CH] = acc[t].astype(jnp.bfloat16)
            rem[which, :, t * CH:(t + 1) * CH] = carry[t]


def attention(qt, kp, vt):
    vmem = pl.BlockSpec(memory_space=pltpu.VMEM)
    return pl.pallas_call(
        attention_kernel,
        out_shape=(jax.ShapeDtypeStruct((2, HEAD_DIM, NT * CH), jnp.bfloat16),
                   jax.ShapeDtypeStruct((2, 8, NT * CH), jnp.float32)),
        in_specs=[vmem] * 3,
        out_specs=(vmem, vmem),
        scratch_shapes=[
            pltpu.VMEM((NT, HEAD_DIM, CH), jnp.float32),
            pltpu.VMEM((NT, 8, CH), jnp.float32),
            pltpu.VMEM((NT, CH, CH), jnp.float32),
            pltpu.VMEM((NT, CH, CH), jnp.float32),
            pltpu.VMEM((NT, CH, CH), jnp.bfloat16),
            pltpu.VMEM((NT, CH, CH), jnp.bfloat16),
        ],
        compiler_params=pltpu.CompilerParams(vmem_limit_bytes=50 * 2**20),
    )(qt, kp, vt)


def strided(rows):
    n = rows.shape[0]
    return rows.reshape(n // CH, 8, CH // 8, -1).transpose(0, 2, 1, 3).reshape(n, -1)


def split_two(x):
    hi = x.astype(jnp.bfloat16)
    return hi, (x - hi.astype(jnp.float32)).astype(jnp.bfloat16)


def per_device(tokens, norm_gain, signal_proj, postgate_proj, pregate_proj, query_proj, key_proj,
               value_proj, filter_taps, break_bias, filter_readout, attention_readout):
    n = tokens.shape[0]
    me = lax.axis_index("sp")
    projections = (signal_proj, postgate_proj, pregate_proj, query_proj, key_proj, value_proj)
    whole_rows = lax.all_gather(tokens, "tp", axis=1, tiled=True)
    widened = whole_rows.astype(jnp.float32)
    inverse = lax.rsqrt(jnp.mean(widened * widened, axis=1) + epsilon)
    scaled = (widened * norm_gain[None, :]).astype(jnp.bfloat16)
    products = [jnp.dot(scaled, w, preferred_element_type=jnp.float32) for w in projections]
    signal, post_gate, pre_gate, queries, keys, values = [
        (p * inverse[:, None]).astype(jnp.bfloat16) for p in products]

    rim = CONV_W - 1
    product = pre_gate.astype(jnp.float32) * signal.astype(jnp.float32)
    before = lax.ppermute(product[n - rim:], "sp", [(i, i + 1) for i in range(15)])
    extended = jnp.concatenate([before, product], axis=0)
    taps = filter_taps.astype(jnp.float32)
    running = sum(taps[w][None, :] * extended[w:w + n] for w in range(CONV_W))
    filtered = (post_gate.astype(jnp.float32) * running).astype(jnp.bfloat16)

    mirror = [(i, 15 - i) for i in range(16)]
    mine = me // 8
    qrows = queries.T.reshape(2, HEAD_DIM, n)
    own_q = lax.dynamic_index_in_dim(qrows, mine, 0, False)
    other_q = lax.ppermute(lax.dynamic_index_in_dim(qrows, 1 - mine, 0, False), "sp", mirror)
    hi, lo = split_two(jnp.stack([own_q, other_q]).astype(jnp.float32) * (HEAD_DIM ** -0.5 * LOG2E))
    ones = jnp.ones((2, 2, n), jnp.bfloat16)
    qt = jnp.concatenate([hi, ones, jnp.zeros((2, 62, n), jnp.bfloat16), lo,
                          jnp.zeros((2, 64, n), jnp.bfloat16)], axis=1)
    bias_hi, bias_lo = split_two(break_bias.astype(jnp.float32) * LOG2E)
    pad = jnp.zeros((n, 62), jnp.bfloat16)
    kp = jnp.stack([strided(jnp.concatenate(
        [keys[:, h * 64:(h + 1) * 64], bias_hi[:, h:h + 1], bias_lo[:, h:h + 1], pad], axis=1))
        for h in range(2)])
    vt = strided(values).reshape(NT, CH, 2, HEAD_DIM).transpose(2, 0, 3, 1)
    all_kp = lax.all_gather(kp, "sp")
    all_vt = lax.all_gather(vt, "sp")
    out, rem = attention(qt, all_kp, all_vt)
    back_out = lax.ppermute(out[1], "sp", mirror)
    back_rem = lax.ppermute(rem[1, :1], "sp", mirror)

    def arranged(own, back):
        return jnp.where(mine == 0, jnp.concatenate([own, back], 0), jnp.concatenate([back, own], 0))

    attended = arranged(out[0], back_out).T
    mass_logarithm = jnp.log(jnp.maximum(1.0 - arranged(rem[0, :1], back_rem), mass_floor))
    filter_rows = lax.all_to_all(filtered, "tp", split_axis=0, concat_axis=1, tiled=True)
    attended_rows = lax.all_to_all(attended, "tp", split_axis=0, concat_axis=1, tiled=True)
    mixed = (jnp.dot(filter_rows, filter_readout, preferred_element_type=jnp.float32)
             + jnp.dot(attended_rows, attention_readout, preferred_element_type=jnp.float32)).astype(jnp.bfloat16)
    return (mixed, mass_logarithm)


def solution(mesh):
    placed = (P("sp", "tp"), P()) + (P(None, "tp"),) * 7 + (P("sp", "tp"), P(), P())
    return jax.shard_map(per_device, mesh=mesh, in_specs=placed,
                         out_specs=(P(("sp", "tp"), None), P("tp", "sp")), check_vma=False)
```

time: 877 us -> 251 us (0.29)
  the two profiles are of different devices: /device:TPU:38 before, /device:TPU:1 now
where the time goes in v1:
time: 251 us; the launch traced here: 250 us
  waiting for transfers between devices  145 us (58%)
  Pallas kernels  37.1 us (15%)
  starting transfers between devices  21.7 us (9%)
  matrix products  21 us (8%)
  between operations  14.1 us (6%)
  other arithmetic  6.09 us (2%)
  local copies, waits for them, and re-layouts  4.74 us (2%)
    all_gather x1, waiting for transfers between devices, per_device(): all_kp = lax.all_gather(kp, 'sp')  73.3 us
    all_gather x1, waiting for transfers between devices, per_device(): whole_rows = lax.all_gather(tokens, 'tp', axis=1, tiled=True)  40.9 us
    pallas_call x1, Pallas kernels, attention(): pl.pallas_call(attention_kernel, out_shape=(jax.ShapeDtypeStruct((2, HEAD...  37.1 us
    all_gather x1, waiting for transfers between devices, per_device(): all_vt = lax.all_gather(vt, 'sp')  24.9 us
    dot_general x6, matrix products, per_device(): jnp.dot(scaled, w, preferred_element_type=jnp.float32)  14.3 us
    all_to_all x1, starting transfers between devices, per_device(): lax.all_to_all(attended, 'tp', split_axis=0, concat_axis=1, tiled=True)  6.02 us
  transfers between devices with their start and end apart: 9, of which 5 were waited for; matrix products, arithmetic and copies ran while one was open for 9% of the time, Pallas kernels for 15%

profile of v1, /device:TPU:1, one launch (start us, length us, event | category | flops | bytes accessed | tf_op | source)
XLA Modules:
  0.0 250.2 jit_solution(2790003400874396441)
XLA Ops:
  7.2 0.0 copy-start
  7.2 0.0 copy-start.10
  7.2 0.0 all-gather.6.cloned.1.call-start
  7.2 0.7 all-gather.6.cloned.1.call-update
  7.9 0.0 all-gather.10.cloned.1.call-start
  8.0 40.9 %all-gather.6.cloned.1.call-done = bf16[1024,2048]{1,0:T(8,128)(2,1)} async-done(((bf16[1024,256]{1,0:T(8,128)(2,1)}), bf16[1024,2048]{1,0:T(8,128)(2,1)}) %all-gather.6.cloned.1.call-update) | async-done | bytes 4194320 | tf_op jit(solution)/shard_map/all_gather | solution.py:151
  48.9 3.2 %fusion.1 = f32[1024]{0:T(1024)S(1)} fusion(bf16[1024,2048]{1,0:T(8,128)(2,1)} %all-gather.6.cloned.1.call-done), kind=kLoop, calls=%fused_computation.3 | loop fusion | flops 6290432 | bytes 4198400 | tf_op jit(solution)/shard_map/reduce_sum | solution.py:153
  52.1 0.0 copy-done
  52.1 0.0 copy-done.10
  52.1 0.2 copy-done.1
  52.3 1.3 fusion.33
  53.6 0.1 copy.70
  53.7 0.2 reshape_reshape.3
  53.9 1.0 copy.63
  54.9 0.0 all-gather.10.cloned.1.call-update
  55.0 0.0 all-gather.8.cloned.1.call-start
  55.0 0.0 copy-done.3
  55.1 0.2 copy.57
  55.3 0.2 copy.56
  55.5 0.2 copy.60
  55.7 0.2 copy.59
  55.9 0.1 pad.17.clone
  56.0 0.0 copy-done.5
  56.0 3.5 %fusion.36 = bf16[1024,128]{1,0:T(8,128)(2,1)S(1)} fusion(bf16[2048,128]{1,0:T(8,128)(2,1)S(1)} %copy-done.5, bf16[1024,2048]{1,0:T(8,128)(2,1)} %all-gather.6.cloned.1.call-done, f32[2048]{0:T(1024)S(1)} %copy-done.10, f32[1024]{0:T(1024)S(1)} %add_rsqrt_fusion), kind=kOutput, calls=%fused_computation.19 | convolution fusion | flops 543424512 | bytes 4993024 | tf_op jit(solution)/shard_map/dot_general | solution.py:155
  59.5 0.0 copy-start.4
  59.5 0.0 copy-start.6
  59.5 0.1 fusion.81
  59.6 0.5 maximum_maximum_fusion
  60.1 0.1 copy.61
  60.3 0.1 copy.58
  60.4 0.8 pad_maximum_fusion.1
  61.2 0.0 all-gather.8.cloned.1.call-update
  61.3 0.0 copy-done.4
  61.3 0.0 copy-done.6
  61.3 0.0 copy-start.7
  61.3 3.6 %fusion.54 = f32[1024,128]{1,0:T(8,128)S(1)} fusion(bf16[2048,128]{1,0:T(8,128)(2,1)S(1)} %copy-done.6, bf16[1024,2048]{1,0:T(8,128)(2,1)} %all-gather.6.cloned.1.call-done, f32[2048]{0:T(1024)S(1)} %copy-done.10, f32[1024]{0:T(1024)S(1)} %add_rsqrt_fusion), kind=kOutput, calls=%fused_computation.25 | convolution fusion | flops 543555584 | bytes 5255168 | tf_op jit(solution)/shard_map/dot_general | solution.py:155
  65.0 0.0 copy-start.8
  65.0 1.3 fusion.48
  66.2 0.0 copy-start.9
  66.2 3.2 %collective-permute-start = (f32[2,128]{1,0:T(2,128)S(1)}, f32[2,128]{1,0:T(2,128)S(1)}, u32[]{:S(2)}, u32[]{:S(2)}) collective-permute-start(f32[2,128]{1,0:T(2,128)S(1)} %slice.64), channel_id=1, source_target_pairs={{0,8},{8,16},{16,24},{24,32},{32,40},{40,48},{48,56},{56,64},{64,7... | collective-permute-start | bytes 3080 | tf_op jit(solution)/shard_map/ppermute | solution.py:161
  69.5 1.3 fusion.63
  70.7 0.1 copy.54
  70.9 3.1 %collective-permute-start.1 = (bf16[64,1024]{1,0:T(8,128)(2,1)S(1)}, bf16[64,1024]{1,0:T(8,128)(2,1)S(1)}, u32[]{:S(2)}, u32[]{:S(2)}) collective-permute-start(bf16[64,1024]{1,0:T(8,128)(2,1)S(1)} %get-tuple-element.13), channel_id=1, source_target_pairs={{0,120},{8,112},{16,104},{24,96},{32,88},{40,80},{48,72},{56,64},{... | collective-permute-start | bytes 393224 | tf_op jit(solution)/shard_map/ppermute | solution.py:171
  74.0 0.0 collective-permute-done
  74.0 3.5 %fusion.71 = bf16[1024,128]{1,0:T(8,128)(2,1)S(1)} fusion(f32[2,128]{1,0:T(2,128)S(1)} %collective-permute-done, f32[1024,128]{1,0:T(8,128)S(1)} %fusion.48, f32[128]{0:T(128)S(1)} %get-tuple-element.23, f32[128]{0:T(128)S(1)} %get-tuple-element.24, f32[128]{0:T(128)S(1)} %get-tuple-element.22, f32[1024]{0:T(1024)S(1)} %add_rsqrt_fusion, ...), kind=kOutput, calls=%fused_computation.36 | convolution fusion | flops 544735232 | bytes 5519872 | tf_op jit(solution)/shard_map/dot_general | solution.py:155
  77.5 0.9 copy.52
  78.4 4.4 %all-to-all-start = ((bf16[8,128,128]{1,2,0:T(8,128)(2,1)}), bf16[8,128,128]{1,2,0:T(8,128)(2,1)S(1)}, u32[]{:S(2)}, u32[]{:S(2)}) async-start(bf16[8,128,128]{1,2,0:T(8,128)(2,1)} %copy.52), calls=%async_computation | async-start | bytes 524288 | tf_op jit(solution)/shard_map/all_to_all | solution.py:193
  82.8 0.0 collective-permute-done.1
  82.8 0.1 subtract_convert_fusion
  83.0 0.7 concatenate.25.qt
  83.7 24.9 %all-gather.10.cloned.1.call-done = bf16[32,4,64,256]{3,2,1,0:T(8,128)(2,1)} async-done(((bf16[2,4,64,256]{3,2,1,0:T(8,128)(2,1)}), bf16[32,4,64,256]{3,2,1,0:T(8,128)(2,1)}) %all-gather.10.cloned.1.call-update) | async-done | bytes 4194320 | tf_op jit(solution)/shard_map/all_gather | solution.py:183
  108.6 73.3 %all-gather.8.cloned.1.call-done = bf16[32,1024,128]{2,1,0:T(8,128)(2,1)} async-done(((bf16[2,1024,128]{2,1,0:T(8,128)(2,1)}), bf16[32,1024,128]{2,1,0:T(8,128)(2,1)}) %all-gather.8.cloned.1.call-update) | async-done | bytes 8388624 | tf_op jit(solution)/shard_map/all_gather | solution.py:182
  181.9 37.1 %shard_map.131 = (bf16[2,64,1024]{2,1,0:T(8,128)(2,1)S(1)}, f32[2,8,1024]{2,1,0:T(8,128)S(1)}) custom-call(bf16[2,256,1024]{2,1,0:T(8,128)(2,1)S(1)} %concatenate.25.qt, bf16[16,2,1024,128]{3,2,1,0:T(8,128)(2,1)} %bitcast.60, bf16[16,2,4,64,256]{4,3,2,1,0:T(8,128)(2,1)} %bitcast.61), custom_call_target="tpu_custom_call" | custom-call | tf_op jit(solution)/shard_map/pallas_call | solution.py:118
  219.1 2.8 %collective-permute-start.2 = (bf16[64,1024]{1,0:T(8,128)(2,1)S(1)}, bf16[64,1024]{1,0:T(8,128)(2,1)S(1)}, u32[]{:S(2)}, u32[]{:S(2)}) collective-permute-start(bf16[64,1024]{1,0:T(8,128)(2,1)S(1)} %get-tuple-element.7), channel_id=1, source_target_pairs={{0,120},{8,112},{16,104},{24,96},{32,88},{40,80},{48,72},{56,64},{... | collective-permute-start | bytes 393224 | tf_op jit(solution)/shard_map/ppermute | solution.py:185
  221.9 2.1 collective-permute-start.3
  224.0 2.7 %collective-permute-done.2 = bf16[64,1024]{1,0:T(8,128)(2,1)S(1)} collective-permute-done((bf16[64,1024]{1,0:T(8,128)(2,1)S(1)}, bf16[64,1024]{1,0:T(8,128)(2,1)S(1)}, u32[]{:S(2)}, u32[]{:S(2)}) %collective-permute-start.2) | collective-permute-done | bytes 131104 | tf_op jit(solution)/shard_map/ppermute | solution.py:185
  226.7 0.8 copy_bitcast_fusion
  227.5 0.0 all-to-all-done
  227.5 6.0 %all-to-all-start.1 = ((bf16[8,128,128]{1,2,0:T(8,128)(2,1)}), bf16[8,128,128]{1,2,0:T(8,128)(2,1)S(1)}, u32[]{:S(2)}, u32[]{:S(2)}) async-start(bf16[8,128,128]{1,2,0:T(8,128)(2,1)} %copy_bitcast_fusion), calls=%async_computation.1 | async-start | bytes 524288 | tf_op jit(solution)/shard_map/all_to_all | solution.py:194
  233.5 2.9 %fusion.84 = f32[128,2048]{1,0:T(8,128)S(1)} fusion(bf16[128,1024]{0,1:T(8,128)(2,1)S(1)} %bitcast.70, bf16[1024,2048]{1,0:T(8,128)(2,1)} %param.22), kind=kOutput, calls=%fused_computation.70 | convolution fusion | flops 536870912 | bytes 5505024 | tf_op jit(solution)/shard_map/dot_general | solution.py:195
  236.4 0.0 collective-permute-done.3
  236.4 0.6 fusion.79
  237.1 2.9 %all-to-all-done.1 = bf16[8,128,128]{1,2,0:T(8,128)(2,1)S(1)} async-done(((bf16[8,128,128]{1,2,0:T(8,128)(2,1)}), bf16[8,128,128]{1,2,0:T(8,128)(2,1)S(1)}, u32[]{:S(2)}, u32[]{:S(2)}) %all-to-all-start.1) | async-done | bytes 262176 | tf_op jit(solution)/shard_map/all_to_all | solution.py:194
  240.0 3.7 %fusion.2 = bf16[128,2048]{1,0:T(8,128)(2,1)} fusion(f32[128,2048]{1,0:T(8,128)S(1)} %fusion.84, bf16[128,1024]{0,1:T(8,128)(2,1)S(1)} %bitcast.63, bf16[1024,2048]{1,0:T(8,128)(2,1)} %param.23), kind=kOutput, calls=%fused_computation.5 | convolution fusion | flops 537395200 | bytes 6029312 | tf_op jit(solution)/shard_map/dot_general | solution.py:196
  (21 shorter events, 0.2 us)
Async XLA Ops:
  7.2 44.9 %copy-start = (bf16[2048,128]{1,0:T(8,128)(2,1)S(1)}, bf16[2048,128]{1,0:T(8,128)(2,1)}, u32[]{:S(2)}) copy-start(bf16[2048,128]{1,0:T(8,128)(2,1)} %param.19) | copy-start | bytes 1572868
  7.2 44.9 %copy-start.10 = (f32[2048]{0:T(1024)S(1)}, f32[2048]{0:T(1024)}, u32[]{:S(2)}) copy-start(f32[2048]{0:T(1024)} %param.13) | copy-start | bytes 24580
  7.2 41.7 %all-gather.6.cloned.1.call-start = ((), (), s32[]{:S(2)}) async-start(), calls=%async_computation.2 | async-start | bytes 4718592 | tf_op jit(solution)/shard_map/all_gather | solution.py:151
  7.9 100.7 %all-gather.10.cloned.1.call-start = ((), (), s32[]{:S(2)}) async-start(), calls=%async_computation.4 | async-start | bytes 4456448 | tf_op jit(solution)/shard_map/all_gather | solution.py:183
  48.8 3.4 %copy-start.1 = (bf16[1024,2048]{1,0:T(8,128)(2,1)S(1)}, bf16[1024,2048]{1,0:T(8,128)(2,1)}, u32[]{:S(2)}) copy-start(bf16[1024,2048]{1,0:T(8,128)(2,1)} %all-gather.6.cloned.1.call-done) | copy-start | bytes 12582916
  52.3 2.7 %copy-start.3 = (bf16[1024,2]{0,1:T(2,128)(2,1)S(1)}, bf16[1024,2]{0,1:T(2,128)(2,1)}, u32[]{:S(2)}) copy-start(bf16[1024,2]{0,1:T(2,128)(2,1)} %param.21) | copy-start | bytes 12292
  52.3 3.7 %copy-start.5 = (bf16[2048,128]{1,0:T(8,128)(2,1)S(1)}, bf16[2048,128]{1,0:T(8,128)(2,1)}, u32[]{:S(2)}) copy-start(bf16[2048,128]{1,0:T(8,128)(2,1)} %param.18) | copy-start | bytes 1572868
  55.0 126.9 %all-gather.8.cloned.1.call-start = ((), (), s32[]{:S(2)}) async-start(), calls=%async_computation.3 | async-start | bytes 8912896 | tf_op jit(solution)/shard_map/all_gather | solution.py:182
  59.5 1.8 copy-start.4
  59.5 1.8 copy-start.6
  61.3 3.6 %copy-start.2 = (bf16[1024,2048]{1,0:T(8,128)(2,1)S(1)}, bf16[1024,2048]{1,0:T(8,128)(2,1)}, u32[]{:S(2)}) copy-start(bf16[1024,2048]{1,0:T(8,128)(2,1)} %all-gather.6.cloned.1.call-done) | copy-start | bytes 12582916
  61.3 3.6 %copy-start.7 = (bf16[2048,128]{1,0:T(8,128)(2,1)S(1)}, bf16[2048,128]{1,0:T(8,128)(2,1)}, u32[]{:S(2)}) copy-start(bf16[2048,128]{1,0:T(8,128)(2,1)} %param.14) | copy-start | bytes 1572868
  65.0 4.5 %copy-start.8 = (bf16[2048,128]{1,0:T(8,128)(2,1)S(1)}, bf16[2048,128]{1,0:T(8,128)(2,1)}, u32[]{:S(2)}) copy-start(bf16[2048,128]{1,0:T(8,128)(2,1)} %param.17) | copy-start | bytes 1572868
  66.2 7.8 %copy-start.9 = (bf16[2048,128]{1,0:T(8,128)(2,1)S(1)}, bf16[2048,128]{1,0:T(8,128)(2,1)}, u32[]{:S(2)}) copy-start(bf16[2048,128]{1,0:T(8,128)(2,1)} %param.15) | copy-start | bytes 1572868
  66.2 7.8 %collective-permute-start = (f32[2,128]{1,0:T(2,128)S(1)}, f32[2,128]{1,0:T(2,128)S(1)}, u32[]{:S(2)}, u32[]{:S(2)}) collective-permute-start(f32[2,128]{1,0:T(2,128)S(1)} %slice.64), channel_id=1, source_target_pairs={{0,8},{8,16},{16,24},{24,32},{32,40},{40,48},{48,56},{56,64},{64,7... | collective-permute-start | bytes 3080 | tf_op jit(solution)/shard_map/ppermute | solution.py:161
  70.9 11.9 %collective-permute-start.1 = (bf16[64,1024]{1,0:T(8,128)(2,1)S(1)}, bf16[64,1024]{1,0:T(8,128)(2,1)S(1)}, u32[]{:S(2)}, u32[]{:S(2)}) collective-permute-start(bf16[64,1024]{1,0:T(8,128)(2,1)S(1)} %get-tuple-element.13), channel_id=1, source_target_pairs={{0,120},{8,112},{16,104},{24,96},{32,88},{40,80},{48,72},{56,64},{... | collective-permute-start | bytes 393224 | tf_op jit(solution)/shard_map/ppermute | solution.py:171
  78.4 149.1 %all-to-all-start = ((bf16[8,128,128]{1,2,0:T(8,128)(2,1)}), bf16[8,128,128]{1,2,0:T(8,128)(2,1)S(1)}, u32[]{:S(2)}, u32[]{:S(2)}) async-start(bf16[8,128,128]{1,2,0:T(8,128)(2,1)} %copy.52), calls=%async_computation | async-start | bytes 524288 | tf_op jit(solution)/shard_map/all_to_all | solution.py:193
  219.1 7.6 %collective-permute-start.2 = (bf16[64,1024]{1,0:T(8,128)(2,1)S(1)}, bf16[64,1024]{1,0:T(8,128)(2,1)S(1)}, u32[]{:S(2)}, u32[]{:S(2)}) collective-permute-start(bf16[64,1024]{1,0:T(8,128)(2,1)S(1)} %get-tuple-element.7), channel_id=1, source_target_pairs={{0,120},{8,112},{16,104},{24,96},{32,88},{40,80},{48,72},{56,64},{... | collective-permute-start | bytes 393224 | tf_op jit(solution)/shard_map/ppermute | solution.py:185
  221.9 14.6 %collective-permute-start.3 = (f32[1,1024]{1,0:T(1,128)S(1)}, f32[1,1024]{1,0:T(1,128)S(1)}, u32[]{:S(2)}, u32[]{:S(2)}) collective-permute-start(f32[1,1024]{1,0:T(1,128)S(1)} %get-tuple-element.15), channel_id=1, source_target_pairs={{0,120},{8,112},{16,104},{24,96},{32,88},{40,80},{48,72},{56,64},{... | collective-permute-start | bytes 12296 | tf_op jit(solution)/shard_map/ppermute | solution.py:186
  227.5 12.5 %all-to-all-start.1 = ((bf16[8,128,128]{1,2,0:T(8,128)(2,1)}), bf16[8,128,128]{1,2,0:T(8,128)(2,1)S(1)}, u32[]{:S(2)}, u32[]{:S(2)}) async-start(bf16[8,128,128]{1,2,0:T(8,128)(2,1)} %copy_bitcast_fusion), calls=%async_computation.1 | async-start | bytes 524288 | tf_op jit(solution)/shard_map/all_to_all | solution.py:194
Sparse Core Ops, SparseCore 0:
  9.7 39.1 all-gather.5
  55.1 53.5 all-gather.9
  111.4 70.5 all-gather.7

commit v2 on v1

--- a/solution.py
+++ b/solution.py
@@ -95,42 +95,241 @@
         acc[t] += jnp.dot(vp, wb[t], preferred_element_type=jnp.float32)
 
 
-def attention_kernel(qt, kp, vt, out, rem, acc, carry, ya, yb, wa, wb):
-    me = lax.axis_index("sp")
-    head = me // 8
+SP, TP = "sp", "tp"
+
+
+def remote(src, dst, send, recv, sp, tp):
+    return pltpu.make_async_remote_copy(src_ref=src, dst_ref=dst, send_sem=send, recv_sem=recv,
+                                        device_id={SP: sp, TP: tp}, device_id_type=pl.DeviceIdType.MESH)
+
+
+def query_place(z, x):
+    flip = (z == 1) | (z == 3)
+    column = jnp.where(flip, 3 - x, x)
+    core = jnp.where((z == 1) | (z == 2), 1, 0)
+    slot = jnp.where((z == 2) | (z == 3), 0, 1)
+    return column, core, slot
+
+
+def set_block(x, core, slot):
+    return jnp.where(core == 0, jnp.where(slot == 0, 15 - x, x), jnp.where(slot == 0, 8 + x, 7 - x))
+
+
+def attention_kernel(q, kp, vt, out, rem, kb, vb, qb, ob, rb, qt, acc, carry, ya, yb, wa, wb,
+                     rk, rv, rq, ro, rr, sk, sv, sq, so, sr, xk, xv, dk, dv, fk):
+    me = lax.axis_index(SP)
+    t = lax.axis_index(TP)
+    z, x = me // 4, me % 4
+    core = t % 2
+    partner = t + 1 - 2 * core
+    active = core == z // 2
+    right = z * 4 + (x + 1) % 4
+    left = z * 4 + (x + 3) % 4
+
+    col, qcore, slot = query_place(z, x)
+    qtp = t - core + qcore
+
+    def key_copy(l):
+        g = 2 * core + l
+        return (remote(kp.at[l], kb.at[me], sk.at[l], rk.at[me], g * 4 + x, t),
+                remote(vt.at[l], vb.at[me], sv.at[l], rv.at[me], g * 4 + x, t))
+
+    def query_copy(l):
+        g = 2 * core + l
+        return remote(q.at[l], qb.at[slot], sq.at[l], rq.at[slot], g * 4 + col, qtp)
+
+    def query_local(l):
+        g = 2 * core + l
+        return (g == z) & (col == x) & (qcore == core)
+
+    for l in range(2):
+        @pl.when(2 * core + l != z)
+        def _():
+            for c in key_copy(l):
+                c.start()
+
+        @pl.when(jnp.logical_not(query_local(l)))
+        def _():
+            query_copy(l).start()
+
+        @pl.when(2 * core + l == z)
+        def _():
+            kb[me] = kp[l]
+            vb[me] = vt[l]
+
+        @pl.when(query_local(l))
+        def _():
+            qb[slot] = q[l]
+
+    def pass_on(b, to, ks, vs, keys=True, values=True, tp=t, src=None):
+        ksrc, vsrc = src or (kb.at[b], vb.at[b])
+        if keys:
+            remote(ksrc, kb.at[b], ks, rk.at[b], to, tp).start()
+        if values:
+            remote(vsrc, vb.at[b], vs, rv.at[b], to, tp).start()
+
+    def sent(b, to, ks, vs, keys=True, values=True, tp=t):
+        if keys:
+            remote(kb.at[b], kb.at[b], ks, rk.at[b], to, tp).wait_send()
+        if values:
+            remote(vb.at[b], vb.at[b], vs, rv.at[b], to, tp).wait_send()
+
+    def arrived(b, keys=True, values=True):
+        if keys:
+            remote(kb.at[b], kb.at[b], sk.at[0], rk.at[b], me, t).wait_recv()
+        if values:
+            remote(vb.at[b], vb.at[b], sv.at[0], rv.at[b], me, t).wait_recv()
+
+    @pl.when(active)
+    def _():
+        for zs in (3, 2, 1, 0):
+            b = zs * 4 + x
+
+            def spread(src):
+                pass_on(b, right, xk.at[zs, 0], xv.at[zs, 0], src=src)
+                pass_on(b, left, xk.at[zs, 1], xv.at[zs, 1], src=src)
+                pass_on(b, me, dk.at[b], dv.at[b], tp=partner, src=src)
+
+            @pl.when(z != zs)
+            def _():
+                arrived(b)
+                spread(None)
+
+            @pl.when(z == zs)
+            def _():
+                spread((kp.at[zs % 2], vt.at[zs % 2]))
+        for zs in (3, 2, 1, 0):
+            even = zs % 2 == 0
+            b = zs * 4 + (x + 3) % 4
+            arrived(b)
+            pass_on(b, right, fk.at[zs, 0], fk.at[zs, 0], keys=even, values=not even)
+            pass_on(b, me, dk.at[b], dv.at[b], tp=partner)
+            b = zs * 4 + (x + 1) % 4
+            arrived(b)
+            pass_on(b, left, fk.at[zs, 1], fk.at[zs, 1], keys=not even, values=even)
+            pass_on(b, me, dk.at[b], dv.at[b], tp=partner)
+        for zs in (3, 2, 1, 0):
+            b = zs * 4 + (x + 2) % 4
+            arrived(b)
+            pass_on(b, me, dk.at[b], dv.at[b], tp=partner)
+
+    @pl.when(jnp.logical_not(active))
+    def _():
+        for b in range(16):
+            arrived(b)
 
     def kchunk(c):
-        return kp[c // NT, head, pl.ds(pl.multiple_of((c % NT) * CH, CH), CH), :]
+        return kb[c // NT, pl.ds(pl.multiple_of((c % NT) * CH, CH), CH), :]
 
     def vchunk(c):
-        return vt[c // NT, head, c % NT]
-
-    for which in range(2):
-        block = me if which == 0 else 15 - me
-        attend_set(qt.at[which], block, kchunk, vchunk, acc, carry, ya, yb, wa, wb)
-        for t in range(NT):
-            out[which, :, t * CH:(t + 1) * CH] = acc[t].astype(jnp.bfloat16)
-            rem[which, :, t * CH:(t + 1) * CH] = carry[t]
-
-
-def attention(qt, kp, vt):
+        return vb[c // NT, c % NT]
+
+    def result_copies(s):
+        blk = set_block(x, core, s)
+        back = t - core + z // 2
+        return (remote(out_local.at[s], ob.at[z % 2], so.at[s], ro.at[z % 2], blk, back),
+                remote(carry_out.at[s], rb.at[z % 2], sr.at[s], rr.at[z % 2], blk, back))
+
+    out_local, carry_out = acc[1], acc[2]
+    sums = acc[0]
+    for s in range(2):
+        blk = set_block(x, core, s)
+        zb, xb = blk // 4, blk % 4
+        own = (blk == me) & (core == z // 2)
+
+        @pl.when(jnp.logical_not(own))
+        def _():
+            remote(qb.at[s], qb.at[s], sq.at[0], rq.at[s], me, t).wait_recv()
+        qs = qb[s].astype(jnp.float32) * (HEAD_DIM ** -0.5 * LOG2E)
+        hi = qs.astype(jnp.bfloat16)
+        qt[0:64] = hi
+        qt[64:128] = jnp.where(lax.broadcasted_iota(jnp.int32, (64, NT * CH), 0) < 2, 1.0, 0.0).astype(jnp.bfloat16)
+        qt[128:192] = (qs - hi.astype(jnp.float32)).astype(jnp.bfloat16)
+        qt[192:256] = jnp.zeros((64, NT * CH), jnp.bfloat16)
+        attend_set(qt, blk, kchunk, vchunk, sums, carry, ya, yb, wa, wb)
+        for i in range(NT):
+            out_local[s, :, i * CH:(i + 1) * CH] = sums[i].astype(jnp.bfloat16)
+            carry_out[s, :, i * CH:(i + 1) * CH] = carry[i]
+
+        @pl.when(jnp.logical_not(own))
+        def _():
+            for c in result_copies(s):
+                c.start()
+
+        @pl.when(own)
+        def _():
+            ob[z % 2] = out_local[s]
+            rb[z % 2] = carry_out[s]
+
+    for l in range(2):
+        @pl.when(jnp.logical_not(query_local(l)))
+        def _():
+            remote(ob.at[l], ob.at[l], so.at[0], ro.at[l], me, t).wait_recv()
+            remote(rb.at[l], rb.at[l], sr.at[0], rr.at[l], me, t).wait_recv()
+        out[l] = ob[l]
+        rem[l] = rb[l]
+
+    for l in range(2):
+        @pl.when(2 * core + l != z)
+        def _():
+            for c in key_copy(l):
+                c.wait_send()
+
+        @pl.when(jnp.logical_not(query_local(l)))
+        def _():
+            query_copy(l).wait_send()
+
+    @pl.when(active)
+    def _():
+        for zs in (3, 2, 1, 0):
+            even = zs % 2 == 0
+            b = zs * 4 + x
+            sent(b, right, xk.at[zs, 0], xv.at[zs, 0])
+            sent(b, left, xk.at[zs, 1], xv.at[zs, 1])
+            sent(zs * 4 + (x + 3) % 4, right, fk.at[zs, 0], fk.at[zs, 0], keys=even, values=not even)
+            sent(zs * 4 + (x + 1) % 4, left, fk.at[zs, 1], fk.at[zs, 1], keys=not even, values=even)
+        for b in range(16):
+            sent(b, me, dk.at[b], dv.at[b], tp=partner)
+
+    for s in range(2):
+        own = (set_block(x, core, s) == me) & (core == z // 2)
+
+        @pl.when(jnp.logical_not(own))
+        def _():
+            for c in result_copies(s):
+                c.wait_send()
+
+
+def attention(q, kp, vt):
     vmem = pl.BlockSpec(memory_space=pltpu.VMEM)
+    rows = NT * CH
+    dma = pltpu.SemaphoreType.DMA
     return pl.pallas_call(
         attention_kernel,
-        out_shape=(jax.ShapeDtypeStruct((2, HEAD_DIM, NT * CH), jnp.bfloat16),
-                   jax.ShapeDtypeStruct((2, 8, NT * CH), jnp.float32)),
+        out_shape=(jax.ShapeDtypeStruct((2, HEAD_DIM, rows), jnp.bfloat16),
+                   jax.ShapeDtypeStruct((2, 8, rows), jnp.float32)),
         in_specs=[vmem] * 3,
         out_specs=(vmem, vmem),
         scratch_shapes=[
-            pltpu.VMEM((NT, HEAD_DIM, CH), jnp.float32),
+            pltpu.VMEM((16, rows, 128), jnp.bfloat16),
+            pltpu.VMEM((16, NT, HEAD_DIM, CH), jnp.bfloat16),
+            pltpu.VMEM((2, HEAD_DIM, rows), jnp.bfloat16),
+            pltpu.VMEM((2, HEAD_DIM, rows), jnp.bfloat16),
+            pltpu.VMEM((2, 8, rows), jnp.float32),
+            pltpu.VMEM((256, rows), jnp.bfloat16),
+            (pltpu.VMEM((NT, HEAD_DIM, CH), jnp.float32), pltpu.VMEM((2, HEAD_DIM, rows), jnp.bfloat16),
+             pltpu.VMEM((2, 8, rows), jnp.float32)),
             pltpu.VMEM((NT, 8, CH), jnp.float32),
             pltpu.VMEM((NT, CH, CH), jnp.float32),
             pltpu.VMEM((NT, CH, CH), jnp.float32),
             pltpu.VMEM((NT, CH, CH), jnp.bfloat16),
             pltpu.VMEM((NT, CH, CH), jnp.bfloat16),
+            dma((16,)), dma((16,)), dma((2,)), dma((2,)), dma((2,)),
+            dma((2,)), dma((2,)), dma((2,)), dma((2,)), dma((2,)),
+            dma((4, 2)), dma((4, 2)), dma((16,)), dma((16,)), dma((4, 2)),
         ],
-        compiler_params=pltpu.CompilerParams(vmem_limit_bytes=50 * 2**20),
-    )(qt, kp, vt)
+        compiler_params=pltpu.CompilerParams(vmem_limit_bytes=50 * 2**20, has_side_effects=True),
+    )(q, kp, vt)
 
 
 def strided(rows):
@@ -146,7 +345,6 @@
 def per_device(tokens, norm_gain, signal_proj, postgate_proj, pregate_proj, query_proj, key_proj,
                value_proj, filter_taps, break_bias, filter_readout, attention_readout):
     n = tokens.shape[0]
-    me = lax.axis_index("sp")
     projections = (signal_proj, postgate_proj, pregate_proj, query_proj, key_proj, value_proj)
     whole_rows = lax.all_gather(tokens, "tp", axis=1, tiled=True)
     widened = whole_rows.astype(jnp.float32)
@@ -164,32 +362,16 @@
     running = sum(taps[w][None, :] * extended[w:w + n] for w in range(CONV_W))
     filtered = (post_gate.astype(jnp.float32) * running).astype(jnp.bfloat16)
 
-    mirror = [(i, 15 - i) for i in range(16)]
-    mine = me // 8
-    qrows = queries.T.reshape(2, HEAD_DIM, n)
-    own_q = lax.dynamic_index_in_dim(qrows, mine, 0, False)
-    other_q = lax.ppermute(lax.dynamic_index_in_dim(qrows, 1 - mine, 0, False), "sp", mirror)
-    hi, lo = split_two(jnp.stack([own_q, other_q]).astype(jnp.float32) * (HEAD_DIM ** -0.5 * LOG2E))
-    ones = jnp.ones((2, 2, n), jnp.bfloat16)
-    qt = jnp.concatenate([hi, ones, jnp.zeros((2, 62, n), jnp.bfloat16), lo,
-                          jnp.zeros((2, 64, n), jnp.bfloat16)], axis=1)
+    q = queries.T.reshape(2, HEAD_DIM, n)
     bias_hi, bias_lo = split_two(break_bias.astype(jnp.float32) * LOG2E)
     pad = jnp.zeros((n, 62), jnp.bfloat16)
     kp = jnp.stack([strided(jnp.concatenate(
         [keys[:, h * 64:(h + 1) * 64], bias_hi[:, h:h + 1], bias_lo[:, h:h + 1], pad], axis=1))
         for h in range(2)])
     vt = strided(values).reshape(NT, CH, 2, HEAD_DIM).transpose(2, 0, 3, 1)
-    all_kp = lax.all_gather(kp, "sp")
-    all_vt = lax.all_gather(vt, "sp")
-    out, rem = attention(qt, all_kp, all_vt)
-    back_out = lax.ppermute(out[1], "sp", mirror)
-    back_rem = lax.ppermute(rem[1, :1], "sp", mirror)
-
-    def arranged(own, back):
-        return jnp.where(mine == 0, jnp.concatenate([own, back], 0), jnp.concatenate([back, own], 0))
-
-    attended = arranged(out[0], back_out).T
-    mass_logarithm = jnp.log(jnp.maximum(1.0 - arranged(rem[0, :1], back_rem), mass_floor))
+    out, rem = attention(q, kp, vt)
+    attended = out.reshape(2 * HEAD_DIM, n).T
+    mass_logarithm = jnp.log(jnp.maximum(1.0 - rem[:, 0], mass_floor))
     filter_rows = lax.all_to_all(filtered, "tp", split_axis=0, concat_axis=1, tiled=True)
     attended_rows = lax.all_to_all(attended, "tp", split_axis=0, concat_axis=1, tiled=True)
     mixed = (jnp.dot(filter_rows, filter_readout, preferred_element_type=jnp.float32)

time: 251 us -> 191 us (0.76)
  waiting for transfers between devices: 145 us -> 47.1 us
  Pallas kernels: 37.1 us -> 91.5 us
  starting transfers between devices: 21.7 us -> 12.1 us
  matrix products: 21 us -> 14.4 us
    all_gather x2 -> x0, waiting for transfers between devices: 98.2 us -> none  [the longest x1 73.3 us: per_device(): all_kp = lax.all_gather(kp, 'sp')]
    pallas_call x1, Pallas kernels: 37.1 us -> 91.5 us  [attention(): pl.pallas_call(attention_kernel, out_shape=(jax.ShapeDtypeStruct((2, HEAD...]
    ppermute x3 -> x0, starting transfers between devices: 7.94 us -> none  [the longest x1 3.07 us: per_device(): lax.ppermute(lax.dynamic_index_in_dim(qrows, 1 - mine, 0, False), 'sp', m...]
    all_to_all x1, waiting for transfers between devices: 0.01 us -> 5.69 us  [per_device(): lax.all_to_all(filtered, 'tp', split_axis=0, concat_axis=1, tiled=True)]
    dot_general x6, matrix products: 14.3 us -> 9.77 us  [per_device(): jnp.dot(scaled, w, preferred_element_type=jnp.float32)]
    ppermute x3 -> x0, waiting for transfers between devices: 2.75 us -> none  [the longest x1 2.74 us: per_device(): back_out = lax.ppermute(out[1], 'sp', mirror)]
  transfers between devices with their start and end apart: 9 -> 4, of which waited for: 5 -> 3; matrix products, arithmetic and copies ran while one was open for 9% -> 6% of each run, Pallas kernels for 15% -> 48%
where the time goes in v2:
time: 191 us; the launch traced here: 190 us
  Pallas kernels  91.5 us (48%)
  waiting for transfers between devices  47.1 us (25%)
  matrix products  14.4 us (8%)
  between operations  14.3 us (7%)
  starting transfers between devices  12.1 us (6%)
  local copies, waits for them, and re-layouts  5.41 us (3%)
  other arithmetic  5.2 us (3%)
    pallas_call x1, Pallas kernels, attention(): pl.pallas_call(attention_kernel, out_shape=(jax.ShapeDtypeStruct((2, HEAD...  91.5 us
    all_gather x1, waiting for transfers between devices, per_device(): whole_rows = lax.all_gather(tokens, 'tp', axis=1, tiled=True)  38.6 us
    dot_general x6, matrix products, per_device(): jnp.dot(scaled, w, preferred_element_type=jnp.float32)  9.77 us
    all_to_all x1, waiting for transfers between devices, per_device(): lax.all_to_all(filtered, 'tp', split_axis=0, concat_axis=1, tiled=True)  5.69 us
    all_to_all x1, starting transfers between devices, per_device(): lax.all_to_all(attended, 'tp', split_axis=0, concat_axis=1, tiled=True)  4.48 us
    all_to_all x1, starting transfers between devices, per_device(): lax.all_to_all(filtered, 'tp', split_axis=0, concat_axis=1, tiled=True)  4.36 us
  transfers between devices with their start and end apart: 4, of which 3 were waited for; matrix products, arithmetic and copies ran while one was open for 6% of the time, Pallas kernels for 48%

profile of v2, /device:TPU:1, one launch (start us, length us, event | category | flops | bytes accessed | tf_op | source)
XLA Modules:
  0.0 190.0 jit_solution(7487561348780545166)
XLA Ops:
  7.2 0.0 copy-start
  7.2 0.0 copy-start.8
  7.2 0.0 all-gather.2.cloned.1.call-start
  7.2 0.7 all-gather.2.cloned.1.call-update
  7.9 0.7 fusion.75
  8.6 0.2 copy.56
  8.8 0.2 copy.57
  9.1 0.2 copy.59
  9.3 0.2 copy.60
  9.5 0.7 convert_element_type.62
  10.2 0.1 pad.9.clone
  10.3 38.6 %all-gather.2.cloned.1.call-done = bf16[1024,2048]{1,0:T(8,128)(2,1)} async-done(((bf16[1024,256]{1,0:T(8,128)(2,1)}), bf16[1024,2048]{1,0:T(8,128)(2,1)}) %all-gather.2.cloned.1.call-update) | async-done | bytes 4194320 | tf_op jit(solution)/shard_map/all_gather | solution.py:349
  48.8 0.0 copy-start.1
  48.9 3.2 %fusion.1 = f32[1024]{0:T(1024)S(1)} fusion(bf16[1024,2048]{1,0:T(8,128)(2,1)} %all-gather.2.cloned.1.call-done), kind=kLoop, calls=%fused_computation.3 | loop fusion | flops 6290432 | bytes 4198400 | tf_op jit(solution)/shard_map/reduce_sum | solution.py:351
  52.1 0.0 copy-done
  52.1 0.0 copy-done.8
  52.1 0.2 copy-done.1
  52.3 1.3 fusion.36
  53.6 0.0 copy-start.3
  53.6 0.1 fusion.76
  53.7 0.5 maximum_maximum_fusion
  54.2 0.1 copy.58
  54.4 0.1 copy.61
  54.5 0.1 copy-done.3
  54.6 0.0 copy-start.4
  54.6 1.3 fusion.54
  55.9 0.0 copy-done.4
  55.9 0.0 copy-start.5
  55.9 1.3 fusion.48
  57.2 0.0 copy-start.6
  57.2 3.2 %collective-permute-start = (f32[2,128]{1,0:T(2,128)S(1)}, f32[2,128]{1,0:T(2,128)S(1)}, u32[]{:S(2)}, u32[]{:S(2)}) collective-permute-start(f32[2,128]{1,0:T(2,128)S(1)} %slice.52), channel_id=1, source_target_pairs={{0,8},{8,16},{16,24},{24,32},{32,40},{40,48},{48,56},{56,64},{64,7... | collective-permute-start | bytes 3080 | tf_op jit(solution)/shard_map/ppermute | solution.py:359
  60.4 0.0 copy-done.5
  60.4 1.3 fusion.33
  61.7 0.0 copy-done.6
  61.7 1.3 fusion.63
  63.0 0.0 copy-start.7
  63.0 0.1 pad_maximum_fusion.1.kp
  63.0 0.1 copy.71
  63.1 0.2 reshape_reshape.3
  63.4 0.4 copy.63
  63.8 0.1 copy.54
  63.9 91.5 %shard_map.131 = (bf16[2,64,1024]{2,1,0:T(8,128)(2,1)S(1)}, f32[2,8,1024]{2,1,0:T(8,128)S(1)}) custom-call(bf16[2,64,1024]{2,1,0:T(8,128)(2,1)S(1)} %bitcast.48, bf16[2,1024,128]{2,1,0:T(8,128)(2,1)S(1)} %pad_maximum_fusion.1.kp, bf16[2,4,64,256]{3,2,1,0:T(8,128)(2,1)S(1)} %bitcast.47), custom_call_target="tpu_custom_call" | custom-call | tf_op jit(solution)/shard_map/pallas_call | solution.py:307
  155.5 0.9 copy.64
  156.3 4.5 %all-to-all-start.1 = ((bf16[8,128,128]{2,1,0:T(8,128)(2,1)}), bf16[8,128,128]{2,1,0:T(8,128)(2,1)S(1)}, u32[]{:S(2)}, u32[]{:S(2)}) async-start(bf16[8,128,128]{2,1,0:T(8,128)(2,1)} %bitcast.19), calls=%async_computation.1 | async-start | bytes 524288 | tf_op jit(solution)/shard_map/all_to_all | solution.py:376
  160.8 0.0 collective-permute-done
  160.8 0.0 copy-done.7
  160.8 3.5 %fusion.71 = bf16[1024,128]{1,0:T(8,128)(2,1)S(1)} fusion(f32[2,128]{1,0:T(2,128)S(1)} %collective-permute-done, f32[1024,128]{1,0:T(8,128)S(1)} %fusion.48, f32[128]{0:T(128)S(1)} %get-tuple-element.15, f32[128]{0:T(128)S(1)} %get-tuple-element.16, f32[128]{0:T(128)S(1)} %get-tuple-element.14, f32[1024]{0:T(1024)S(1)} %add_rsqrt_fusion, ...), kind=kOutput, calls=%fused_computation.36 | convolution fusion | flops 544735232 | bytes 5519872 | tf_op jit(solution)/shard_map/dot_general | solution.py:353
  164.3 0.9 copy.52
  165.1 2.1 %all-to-all-done.1 = bf16[8,128,128]{2,1,0:T(8,128)(2,1)S(1)} async-done(((bf16[8,128,128]{2,1,0:T(8,128)(2,1)}), bf16[8,128,128]{2,1,0:T(8,128)(2,1)S(1)}, u32[]{:S(2)}, u32[]{:S(2)}) %all-to-all-start.1) | async-done | bytes 262176 | tf_op jit(solution)/shard_map/all_to_all | solution.py:376
  167.3 4.4 %all-to-all-start = ((bf16[8,128,128]{1,2,0:T(8,128)(2,1)}), bf16[8,128,128]{1,2,0:T(8,128)(2,1)S(1)}, u32[]{:S(2)}, u32[]{:S(2)}) async-start(bf16[8,128,128]{1,2,0:T(8,128)(2,1)} %copy.52), calls=%async_computation | async-start | bytes 524288 | tf_op jit(solution)/shard_map/all_to_all | solution.py:375
  171.7 0.6 copy.72
  172.3 0.2 copy.65
  172.4 5.7 %all-to-all-done = bf16[8,128,128]{1,2,0:T(8,128)(2,1)S(1)} async-done(((bf16[8,128,128]{1,2,0:T(8,128)(2,1)}), bf16[8,128,128]{1,2,0:T(8,128)(2,1)S(1)}, u32[]{:S(2)}, u32[]{:S(2)}) %all-to-all-start) | async-done | bytes 262176 | tf_op jit(solution)/shard_map/all_to_all | solution.py:375
  178.1 0.0 copy-start.2
  178.1 3.1 %fusion.79 = f32[128,2048]{1,0:T(8,128)S(1)} fusion(bf16[128,1024]{0,1:T(8,128)(2,1)S(1)} %bitcast.57, bf16[1024,2048]{1,0:T(8,128)(2,1)} %param.22), kind=kOutput, calls=%fused_computation.55 | convolution fusion | flops 536870912 | bytes 5505024 | tf_op jit(solution)/shard_map/dot_general | solution.py:377
  181.2 0.4 copy-done.2
  181.6 1.5 fusion.2
  (6 shorter events, 0.1 us)
Async XLA Ops:
  7.2 44.9 %copy-start = (bf16[2048,128]{1,0:T(8,128)(2,1)S(1)}, bf16[2048,128]{1,0:T(8,128)(2,1)}, u32[]{:S(2)}) copy-start(bf16[2048,128]{1,0:T(8,128)(2,1)} %param.18) | copy-start | bytes 1572868
  7.2 44.9 %copy-start.8 = (f32[2048]{0:T(1024)S(1)}, f32[2048]{0:T(1024)}, u32[]{:S(2)}) copy-start(f32[2048]{0:T(1024)} %param.13) | copy-start | bytes 24580
  7.2 41.7 %all-gather.2.cloned.1.call-start = ((), (), s32[]{:S(2)}) async-start(), calls=%async_computation.2 | async-start | bytes 4718592 | tf_op jit(solution)/shard_map/all_gather | solution.py:349
  48.8 3.4 %copy-start.1 = (bf16[1024,2048]{1,0:T(8,128)(2,1)S(1)}, bf16[1024,2048]{1,0:T(8,128)(2,1)}, u32[]{:S(2)}) copy-start(bf16[1024,2048]{1,0:T(8,128)(2,1)} %all-gather.2.cloned.1.call-done) | copy-start | bytes 12582916
  53.6 1.0 copy-start.3
  54.6 1.3 copy-start.4
  55.9 4.5 %copy-start.5 = (bf16[2048,128]{1,0:T(8,128)(2,1)S(1)}, bf16[2048,128]{1,0:T(8,128)(2,1)}, u32[]{:S(2)}) copy-start(bf16[2048,128]{1,0:T(8,128)(2,1)} %param.19) | copy-start | bytes 1572868
  57.2 4.5 %copy-start.6 = (bf16[2048,128]{1,0:T(8,128)(2,1)S(1)}, bf16[2048,128]{1,0:T(8,128)(2,1)}, u32[]{:S(2)}) copy-start(bf16[2048,128]{1,0:T(8,128)(2,1)} %param.17) | copy-start | bytes 1572868
  57.2 103.6 %collective-permute-start = (f32[2,128]{1,0:T(2,128)S(1)}, f32[2,128]{1,0:T(2,128)S(1)}, u32[]{:S(2)}, u32[]{:S(2)}) collective-permute-start(f32[2,128]{1,0:T(2,128)S(1)} %slice.52), channel_id=1, source_target_pairs={{0,8},{8,16},{16,24},{24,32},{32,40},{40,48},{48,56},{56,64},{64,7... | collective-permute-start | bytes 3080 | tf_op jit(solution)/shard_map/ppermute | solution.py:359
  63.0 97.9 %copy-start.7 = (bf16[2048,128]{1,0:T(8,128)(2,1)S(1)}, bf16[2048,128]{1,0:T(8,128)(2,1)}, u32[]{:S(2)}) copy-start(bf16[2048,128]{1,0:T(8,128)(2,1)} %param.15) | copy-start | bytes 1572868
  156.3 11.0 %all-to-all-start.1 = ((bf16[8,128,128]{2,1,0:T(8,128)(2,1)}), bf16[8,128,128]{2,1,0:T(8,128)(2,1)S(1)}, u32[]{:S(2)}, u32[]{:S(2)}) async-start(bf16[8,128,128]{2,1,0:T(8,128)(2,1)} %bitcast.19), calls=%async_computation.1 | async-start | bytes 524288 | tf_op jit(solution)/shard_map/all_to_all | solution.py:376
  167.3 10.9 %all-to-all-start = ((bf16[8,128,128]{1,2,0:T(8,128)(2,1)}), bf16[8,128,128]{1,2,0:T(8,128)(2,1)S(1)}, u32[]{:S(2)}, u32[]{:S(2)}) async-start(bf16[8,128,128]{1,2,0:T(8,128)(2,1)} %copy.52), calls=%async_computation | async-start | bytes 524288 | tf_op jit(solution)/shard_map/all_to_all | solution.py:375
  178.1 3.4 %copy-start.2 = (bf16[1024,2048]{1,0:T(8,128)(2,1)S(1)}, bf16[1024,2048]{1,0:T(8,128)(2,1)}, u32[]{:S(2)}) copy-start(bf16[1024,2048]{1,0:T(8,128)(2,1)} %param.23) | copy-start | bytes 12582916
Sparse Core Ops, SparseCore 0:
  9.7 39.1 all-gather.1

commit v3 on v2

--- a/solution.py
+++ b/solution.py
@@ -96,6 +96,7 @@
 
 
 SP, TP = "sp", "tp"
+ROWS = NT * CH
 
 
 def remote(src, dst, send, recv, sp, tp):
@@ -104,8 +105,7 @@
 
 
 def query_place(z, x):
-    flip = (z == 1) | (z == 3)
-    column = jnp.where(flip, 3 - x, x)
+    column = jnp.where((z == 1) | (z == 3), 3 - x, x)
     core = jnp.where((z == 1) | (z == 2), 1, 0)
     slot = jnp.where((z == 2) | (z == 3), 0, 1)
     return column, core, slot
@@ -115,17 +115,132 @@
     return jnp.where(core == 0, jnp.where(slot == 0, 15 - x, x), jnp.where(slot == 0, 8 + x, 7 - x))
 
 
-def attention_kernel(q, kp, vt, out, rem, kb, vb, qb, ob, rb, qt, acc, carry, ya, yb, wa, wb,
-                     rk, rv, rq, ro, rr, sk, sv, sq, so, sr, xk, xv, dk, dv, fk):
+def layer_kernel(tokens, gain, w0, w1, w2, w3, w4, w5, taps, bias, fr_hbm, ar_hbm, mixed, mass,
+                 tk, wts, fr, ar, sc, pr, post, fl, q, kp, vt, kb, vb, qb, rb, fa, at, total,
+                 qt, out_local, carry_out, sums, carry, ya, yb, wa, wb,
+                 lw, st, rt, sf, rim,
+                 rk, rv, rq, ro, rr, sk, sv, sq, so, sr, xk, xv, dk, dv, fk, sx, rx):
     me = lax.axis_index(SP)
     t = lax.axis_index(TP)
     z, x = me // 4, me % 4
     core = t % 2
+    y = t // 2
     partner = t + 1 - 2 * core
     active = core == z // 2
     right = z * 4 + (x + 1) % 4
     left = z * 4 + (x + 3) % 4
 
+    local = [pltpu.make_async_copy(w, wts.at[:, i * 128:(i + 1) * 128], lw.at[i])
+             for i, w in enumerate((w0, w1, w2, w3, w4, w5))]
+    local += [pltpu.make_async_copy(fr_hbm, fr, lw.at[6]), pltpu.make_async_copy(ar_hbm, ar, lw.at[7])]
+
+    up = (t + 2) % 8
+    down = (t + 6) % 8
+    far = (t + 4) % 8
+
+    def rows(k):
+        return pl.ds(k * CH, CH)
+
+    def feature_sends(k):
+        src = tokens.at[rows(k)]
+        dst = tk.at[t, rows(k)]
+        return [remote(src, dst, st.at[k, 0], rt.at[t, k], me, up),
+                remote(src, dst, st.at[k, 1], rt.at[t, k], me, down),
+                remote(src, dst, st.at[k, 2], rt.at[t, k], me, partner)]
+
+    def relay(k):
+        slot, to = (down, up) if k % 2 == 0 else (up, down)
+        part = tk.at[slot, rows(k)]
+        return remote(part, part, st.at[k, 3], rt.at[slot, k], me, to)
+
+    def over(k, n, slot):
+        part = tk.at[slot, rows(k)]
+        return remote(part, part, st.at[k, 4 + n], rt.at[slot, k], me, partner)
+
+    def got(slot, k):
+        part = tk.at[slot, rows(k)]
+        remote(part, part, st.at[k, 0], rt.at[slot, k], me, t).wait_recv()
+
+    def near(k):
+        got(down, k)
+        got(up, k)
+        relay(k).start()
+        over(k, 0, down).start()
+        over(k, 1, up).start()
+        if k + 2 < NT:
+            for c in feature_sends(k + 2):
+                c.start()
+
+    def rest(k):
+        got(far, k)
+        over(k, 2, far).start()
+        for n in (0, 2, 4, 6):
+            got((partner + n) % 8, k)
+
+    rowi = lax.broadcasted_iota(jnp.int32, (CH, CH), 0)
+    coli = lax.broadcasted_iota(jnp.int32, (CH, CH), 1)
+    order = jnp.where(coli == (rowi % 8) * (CH // 8) + rowi // 8, 1.0, 0.0).astype(jnp.bfloat16)
+    lane = lax.broadcasted_iota(jnp.int32, (CH, 128), 1)
+
+    def project(k):
+        r = rows(k)
+        squares = jnp.zeros((CH, 128), jnp.float32)
+        for s in range(8):
+            v = tk[s, r, :].astype(jnp.float32)
+            v2 = v * v
+            squares = squares + v2[:, :128] + v2[:, 128:]
+            sc[:, s * 256:(s + 1) * 256] = (v * gain[:, s * 256:(s + 1) * 256]).astype(jnp.bfloat16)
+        inverse = lax.rsqrt(jnp.sum(squares, axis=1, keepdims=True) * (1.0 / 2048.0) + epsilon)
+
+        def product(n):
+            p = jnp.dot(sc[...], wts[:, n * 256:(n + 1) * 256], preferred_element_type=jnp.float32)
+            p = (p * inverse).astype(jnp.bfloat16)
+            return p[:, :128], p[:, 128:]
+
+        signal, post_gate = product(0)
+        pre_gate, queries = product(1)
+        keys, values = product(2)
+        pr[8 + k * CH:8 + (k + 1) * CH, :] = pre_gate.astype(jnp.float32) * signal.astype(jnp.float32)
+        post[r, :] = post_gate
+        q[:, r] = queries.astype(jnp.float32).T.astype(jnp.bfloat16)
+        b = bias[r, :].astype(jnp.float32) * LOG2E
+        wide = []
+        for l in range(2):
+            bl = b[:, l:l + 1]
+            hi = bl.astype(jnp.bfloat16).astype(jnp.float32)
+            kf = keys.astype(jnp.float32)
+            if l == 1:
+                kf = pltpu.roll(kf, 64, 1)
+            extra = jnp.where(lane == 64, hi, jnp.where(lane == 65, bl - hi, 0.0))
+            wide.append(jnp.where(lane < 64, kf, extra).astype(jnp.bfloat16))
+        kk = jnp.dot(order, jnp.concatenate(wide, axis=1), preferred_element_type=jnp.float32).astype(jnp.bfloat16)
+        kp[0, r, :] = kk[:, :128]
+        kp[1, r, :] = kk[:, 128:]
+        vv = jnp.dot(order, values, preferred_element_type=jnp.float32).T.astype(jnp.bfloat16)
+        vt[0, k] = vv[:64]
+        vt[1, k] = vv[64:]
+
+    for k in range(2):
+        for c in feature_sends(k):
+            c.start()
+    for c in local:
+        c.start()
+    tk[t] = tokens[...]
+    near(0)
+    near(1)
+    rest(0)
+    for c in local[:6]:
+        c.wait()
+    project(0)
+    near(2)
+    rest(1)
+    project(1)
+    near(3)
+    rest(2)
+    project(2)
+    rest(3)
+    project(3)
+
     col, qcore, slot = query_place(z, x)
     qtp = t - core + qcore
 
@@ -136,7 +251,7 @@
 
     def query_copy(l):
         g = 2 * core + l
-        return remote(q.at[l], qb.at[slot], sq.at[l], rq.at[slot], g * 4 + col, qtp)
+        return remote(q.at[pl.ds(l * 64, 64)], qb.at[slot], sq.at[l], rq.at[slot], g * 4 + col, qtp)
 
     def query_local(l):
         g = 2 * core + l
@@ -159,7 +274,14 @@
 
         @pl.when(query_local(l))
         def _():
-            qb[slot] = q[l]
+            qb[slot] = q[l * 64:(l + 1) * 64, :]
+
+    def rim_copy():
+        return remote(pr.at[pl.ds(ROWS, 8)], pr.at[pl.ds(0, 8)], rim.at[0], rim.at[1], (me + 1) % 16, t)
+
+    @pl.when(me < 15)
+    def _():
+        rim_copy().start()
 
     def pass_on(b, to, ks, vs, keys=True, values=True, tp=t, src=None):
         ksrc, vsrc = src or (kb.at[b], vb.at[b])
@@ -174,11 +296,9 @@
         if values:
             remote(vb.at[b], vb.at[b], vs, rv.at[b], to, tp).wait_send()
 
-    def arrived(b, keys=True, values=True):
-        if keys:
-            remote(kb.at[b], kb.at[b], sk.at[0], rk.at[b], me, t).wait_recv()
-        if values:
-            remote(vb.at[b], vb.at[b], sv.at[0], rv.at[b], me, t).wait_recv()
+    def arrived(b):
+        remote(kb.at[b], kb.at[b], sk.at[0], rk.at[b], me, t).wait_recv()
+        remote(vb.at[b], vb.at[b], sv.at[0], rv.at[b], me, t).wait_recv()
 
     @pl.when(active)
     def _():
@@ -198,6 +318,37 @@
             @pl.when(z == zs)
             def _():
                 spread((kp.at[zs % 2], vt.at[zs % 2]))
+
+    @pl.when(me == 0)
+    def _():
+        pr[0:8, :] = jnp.zeros((8, 128), jnp.float32)
+
+    @pl.when(me > 0)
+    def _():
+        rim_copy().wait_recv()
+    tp_values = taps[...].astype(jnp.float32)
+    running = jnp.zeros((ROWS, 128), jnp.float32)
+    for w in range(CONV_W):
+        running = running + tp_values[w:w + 1, :] * pr[6 + w:6 + w + ROWS, :]
+    fl[...] = (post[...].astype(jnp.float32) * running).astype(jnp.bfloat16)
+
+    @pl.when(me < 15)
+    def _():
+        rim_copy().wait_send()
+
+    def lanes(i):
+        return pl.ds(pl.multiple_of(i * 128, 128), 128)
+
+    def filter_copy(n):
+        p = (t + n) % 8
+        return remote(fl.at[lanes(p)], fa.at[:, lanes(t)], sf.at[n], sf.at[8 + n], me, p)
+
+    for n in range(1, 8):
+        filter_copy(n).start()
+    fa[:, lanes(t)] = fl[lanes(t), :]
+
+    @pl.when(active)
+    def _():
         for zs in (3, 2, 1, 0):
             even = zs % 2 == 0
             b = zs * 4 + (x + 3) % 4
@@ -224,17 +375,18 @@
     def vchunk(c):
         return vb[c // NT, c % NT]
 
-    def result_copies(s):
-        blk = set_block(x, core, s)
-        back = t - core + z // 2
-        return (remote(out_local.at[s], ob.at[z % 2], so.at[s], ro.at[z % 2], blk, back),
-                remote(carry_out.at[s], rb.at[z % 2], sr.at[s], rr.at[z % 2], blk, back))
-
-    out_local, carry_out = acc[1], acc[2]
-    sums = acc[0]
+    back = t - core + z // 2
+    head_rows = pl.ds(pl.multiple_of((4 * y + z) * 64, 64), 64)
+
+    def piece_copy(s, blk, p):
+        return remote(out_local.at[s, :, pl.ds(p * 128, 128)], at.at[head_rows], so.at[s, p],
+                      ro.at[4 * y + z], blk, p)
+
+    def rem_copy(s, blk):
+        return remote(carry_out.at[s], rb.at[z % 2], sr.at[s], rr.at[z % 2], blk, back)
+
     for s in range(2):
         blk = set_block(x, core, s)
-        zb, xb = blk // 4, blk % 4
         own = (blk == me) & (core == z // 2)
 
         @pl.when(jnp.logical_not(own))
@@ -243,32 +395,66 @@
         qs = qb[s].astype(jnp.float32) * (HEAD_DIM ** -0.5 * LOG2E)
         hi = qs.astype(jnp.bfloat16)
         qt[0:64] = hi
-        qt[64:128] = jnp.where(lax.broadcasted_iota(jnp.int32, (64, NT * CH), 0) < 2, 1.0, 0.0).astype(jnp.bfloat16)
+        qt[64:128] = jnp.where(lax.broadcasted_iota(jnp.int32, (64, ROWS), 0) < 2, 1.0, 0.0).astype(jnp.bfloat16)
         qt[128:192] = (qs - hi.astype(jnp.float32)).astype(jnp.bfloat16)
-        qt[192:256] = jnp.zeros((64, NT * CH), jnp.bfloat16)
+        qt[192:256] = jnp.zeros((64, ROWS), jnp.bfloat16)
         attend_set(qt, blk, kchunk, vchunk, sums, carry, ya, yb, wa, wb)
         for i in range(NT):
             out_local[s, :, i * CH:(i + 1) * CH] = sums[i].astype(jnp.bfloat16)
             carry_out[s, :, i * CH:(i + 1) * CH] = carry[i]
+        for p in range(8):
+            here = (blk == me) & (t == p)
+
+            @pl.when(jnp.logical_not(here))
+            def _():
+                piece_copy(s, blk, p).start()
+
+            @pl.when(here)
+            def _():
+                at[head_rows, :] = out_local[s, :, p * 128:(p + 1) * 128]
 
         @pl.when(jnp.logical_not(own))
         def _():
-            for c in result_copies(s):
-                c.start()
+            rem_copy(s, blk).start()
 
         @pl.when(own)
         def _():
-            ob[z % 2] = out_local[s]
             rb[z % 2] = carry_out[s]
 
+    for n in range(1, 8):
+        remote(fl.at[lanes(0)], fa.at[:, lanes((t - n + 8) % 8)], sf.at[n], sf.at[8 + n], me, t).wait_recv()
+    local[6].wait()
+    local[7].wait()
+    for n in range(8):
+        c = slice(n * 256, (n + 1) * 256)
+        total[:, c] = jnp.dot(fa[...], fr[:, c], preferred_element_type=jnp.float32)
+    for h in range(16):
+        hz = h % 4
+        column, hcore, _ = query_place(z, x)
+        mine = (hz == z) & (column == x) & (2 * (h // 4) + hcore == t)
+
+        @pl.when(jnp.logical_not(mine))
+        def _():
+            part = at.at[pl.ds(h * 64, 64)]
+            remote(part, part, so.at[0, 0], ro.at[h], me, t).wait_recv()
+    rows_t = at[...].astype(jnp.float32).T.astype(jnp.bfloat16)
+    for n in range(8):
+        c = slice(n * 256, (n + 1) * 256)
+        mixed[:, c] = (total[:, c] + jnp.dot(rows_t, ar[:, c], preferred_element_type=jnp.float32)).astype(jnp.bfloat16)
     for l in range(2):
         @pl.when(jnp.logical_not(query_local(l)))
         def _():
-            remote(ob.at[l], ob.at[l], so.at[0], ro.at[l], me, t).wait_recv()
             remote(rb.at[l], rb.at[l], sr.at[0], rr.at[l], me, t).wait_recv()
-        out[l] = ob[l]
-        rem[l] = rb[l]
-
+        mass[l:l + 1, :] = jnp.log(jnp.maximum(1.0 - rb[l, 0:1, :], mass_floor))
+
+    for k in range(NT):
+        for c in feature_sends(k):
+            c.wait_send()
+        relay(k).wait_send()
+        for n, sl in enumerate((down, up, far)):
+            over(k, n, sl).wait_send()
+    for n in range(1, 8):
+        filter_copy(n).wait_send()
     for l in range(2):
         @pl.when(2 * core + l != z)
         def _():
@@ -292,91 +478,65 @@
             sent(b, me, dk.at[b], dv.at[b], tp=partner)
 
     for s in range(2):
-        own = (set_block(x, core, s) == me) & (core == z // 2)
+        blk = set_block(x, core, s)
+        own = (blk == me) & (core == z // 2)
+        for p in range(8):
+            @pl.when(jnp.logical_not((blk == me) & (t == p)))
+            def _():
+                piece_copy(s, blk, p).wait_send()
 
         @pl.when(jnp.logical_not(own))
         def _():
-            for c in result_copies(s):
-                c.wait_send()
-
-
-def attention(q, kp, vt):
+            rem_copy(s, blk).wait_send()
+
+
+def per_device(tokens, norm_gain, signal_proj, postgate_proj, pregate_proj, query_proj, key_proj,
+               value_proj, filter_taps, break_bias, filter_readout, attention_readout):
     vmem = pl.BlockSpec(memory_space=pltpu.VMEM)
-    rows = NT * CH
+    hbm = pl.BlockSpec(memory_space=pl.ANY)
     dma = pltpu.SemaphoreType.DMA
+    bf16, f32 = jnp.bfloat16, jnp.float32
     return pl.pallas_call(
-        attention_kernel,
-        out_shape=(jax.ShapeDtypeStruct((2, HEAD_DIM, rows), jnp.bfloat16),
-                   jax.ShapeDtypeStruct((2, 8, rows), jnp.float32)),
-        in_specs=[vmem] * 3,
+        layer_kernel,
+        out_shape=(jax.ShapeDtypeStruct((128, 2048), bf16), jax.ShapeDtypeStruct((2, ROWS), f32)),
+        in_specs=[vmem, vmem] + [hbm] * 6 + [vmem, vmem, hbm, hbm],
         out_specs=(vmem, vmem),
         scratch_shapes=[
-            pltpu.VMEM((16, rows, 128), jnp.bfloat16),
-            pltpu.VMEM((16, NT, HEAD_DIM, CH), jnp.bfloat16),
-            pltpu.VMEM((2, HEAD_DIM, rows), jnp.bfloat16),
-            pltpu.VMEM((2, HEAD_DIM, rows), jnp.bfloat16),
-            pltpu.VMEM((2, 8, rows), jnp.float32),
-            pltpu.VMEM((256, rows), jnp.bfloat16),
-            (pltpu.VMEM((NT, HEAD_DIM, CH), jnp.float32), pltpu.VMEM((2, HEAD_DIM, rows), jnp.bfloat16),
-             pltpu.VMEM((2, 8, rows), jnp.float32)),
-            pltpu.VMEM((NT, 8, CH), jnp.float32),
-            pltpu.VMEM((NT, CH, CH), jnp.float32),
-            pltpu.VMEM((NT, CH, CH), jnp.float32),
-            pltpu.VMEM((NT, CH, CH), jnp.bfloat16),
-            pltpu.VMEM((NT, CH, CH), jnp.bfloat16),
-            dma((16,)), dma((16,)), dma((2,)), dma((2,)), dma((2,)),
-            dma((2,)), dma((2,)), dma((2,)), dma((2,)), dma((2,)),
-            dma((4, 2)), dma((4, 2)), dma((16,)), dma((16,)), dma((4, 2)),
+            pltpu.VMEM((8, ROWS, 256), bf16),
+            pltpu.VMEM((2048, 768), bf16),
+            pltpu.VMEM((1024, 2048), bf16),
+            pltpu.VMEM((1024, 2048), bf16),
+            pltpu.VMEM((CH, 2048), bf16),
+            pltpu.VMEM((ROWS + 8, 128), f32),
+            pltpu.VMEM((ROWS, 128), bf16),
+            pltpu.VMEM((ROWS, 128), bf16),
+            pltpu.VMEM((128, ROWS), bf16),
+            pltpu.VMEM((2, ROWS, 128), bf16),
+            pltpu.VMEM((2, NT, 64, CH), bf16),
+            pltpu.VMEM((16, ROWS, 128), bf16),
+            pltpu.VMEM((16, NT, 64, CH), bf16),
+            pltpu.VMEM((2, 64, ROWS), bf16),
+            pltpu.VMEM((2, 8, ROWS), f32),
+            pltpu.VMEM((128, 1024), bf16),
+            pltpu.VMEM((1024, 128), bf16),
+            pltpu.VMEM((128, 2048), f32),
+            pltpu.VMEM((256, ROWS), bf16),
+            pltpu.VMEM((2, 64, ROWS), bf16),
+            pltpu.VMEM((2, 8, ROWS), f32),
+            pltpu.VMEM((NT, 64, CH), f32),
+            pltpu.VMEM((NT, 8, CH), f32),
+            pltpu.VMEM((NT, CH, CH), f32),
+            pltpu.VMEM((NT, CH, CH), f32),
+            pltpu.VMEM((NT, CH, CH), bf16),
+            pltpu.VMEM((NT, CH, CH), bf16),
+            dma((8,)), dma((4, 8)), dma((8, 4)), dma((16,)), dma((2,)),
+            dma((16,)), dma((16,)), dma((2,)), dma((16,)), dma((2,)),
+            dma((2,)), dma((2,)), dma((2,)), dma((2, 8)), dma((2,)),
+            dma((4, 2)), dma((4, 2)), dma((16,)), dma((16,)), dma((4, 2)), dma((2,)), dma((2,)),
         ],
-        compiler_params=pltpu.CompilerParams(vmem_limit_bytes=50 * 2**20, has_side_effects=True),
-    )(q, kp, vt)
-
-
-def strided(rows):
-    n = rows.shape[0]
-    return rows.reshape(n // CH, 8, CH // 8, -1).transpose(0, 2, 1, 3).reshape(n, -1)
-
-
-def split_two(x):
-    hi = x.astype(jnp.bfloat16)
-    return hi, (x - hi.astype(jnp.float32)).astype(jnp.bfloat16)
-
-
-def per_device(tokens, norm_gain, signal_proj, postgate_proj, pregate_proj, query_proj, key_proj,
-               value_proj, filter_taps, break_bias, filter_readout, attention_readout):
-    n = tokens.shape[0]
-    projections = (signal_proj, postgate_proj, pregate_proj, query_proj, key_proj, value_proj)
-    whole_rows = lax.all_gather(tokens, "tp", axis=1, tiled=True)
-    widened = whole_rows.astype(jnp.float32)
-    inverse = lax.rsqrt(jnp.mean(widened * widened, axis=1) + epsilon)
-    scaled = (widened * norm_gain[None, :]).astype(jnp.bfloat16)
-    products = [jnp.dot(scaled, w, preferred_element_type=jnp.float32) for w in projections]
-    signal, post_gate, pre_gate, queries, keys, values = [
-        (p * inverse[:, None]).astype(jnp.bfloat16) for p in products]
-
-    rim = CONV_W - 1
-    product = pre_gate.astype(jnp.float32) * signal.astype(jnp.float32)
-    before = lax.ppermute(product[n - rim:], "sp", [(i, i + 1) for i in range(15)])
-    extended = jnp.concatenate([before, product], axis=0)
-    taps = filter_taps.astype(jnp.float32)
-    running = sum(taps[w][None, :] * extended[w:w + n] for w in range(CONV_W))
-    filtered = (post_gate.astype(jnp.float32) * running).astype(jnp.bfloat16)
-
-    q = queries.T.reshape(2, HEAD_DIM, n)
-    bias_hi, bias_lo = split_two(break_bias.astype(jnp.float32) * LOG2E)
-    pad = jnp.zeros((n, 62), jnp.bfloat16)
-    kp = jnp.stack([strided(jnp.concatenate(
-        [keys[:, h * 64:(h + 1) * 64], bias_hi[:, h:h + 1], bias_lo[:, h:h + 1], pad], axis=1))
-        for h in range(2)])
-    vt = strided(values).reshape(NT, CH, 2, HEAD_DIM).transpose(2, 0, 3, 1)
-    out, rem = attention(q, kp, vt)
-    attended = out.reshape(2 * HEAD_DIM, n).T
-    mass_logarithm = jnp.log(jnp.maximum(1.0 - rem[:, 0], mass_floor))
-    filter_rows = lax.all_to_all(filtered, "tp", split_axis=0, concat_axis=1, tiled=True)
-    attended_rows = lax.all_to_all(attended, "tp", split_axis=0, concat_axis=1, tiled=True)
-    mixed = (jnp.dot(filter_rows, filter_readout, preferred_element_type=jnp.float32)
-             + jnp.dot(attended_rows, attention_readout, preferred_element_type=jnp.float32)).astype(jnp.bfloat16)
-    return (mixed, mass_logarithm)
+        compiler_params=pltpu.CompilerParams(vmem_limit_bytes=60 * 2**20, has_side_effects=True),
+    )(tokens, norm_gain.reshape(1, -1), signal_proj, postgate_proj, pregate_proj, query_proj, key_proj,
+      value_proj, filter_taps, break_bias, filter_readout, attention_readout)
 
 
 def solution(mesh):

time: 191 us -> 132 us (0.69)
  waiting for transfers between devices: 47.1 us -> 0 us
  Pallas kernels: 91.5 us -> 126 us
  matrix products: 14.4 us -> 0 us
  between operations: 14.3 us -> 0.64 us
  starting transfers between devices: 12.1 us -> 0 us
  other arithmetic: 5.2 us -> 0 us
    all_gather x1 -> x0, waiting for transfers between devices: 38.6 us -> none  [per_device(): whole_rows = lax.all_gather(tokens, 'tp', axis=1, tiled=True)]
    pallas_call x1, Pallas kernels: 91.5 us -> 126 us  [per_device(): pl.pallas_call(layer_kernel, out_shape=(jax.ShapeDtypeStruct((128, 2048),...]
    dot_general x8 -> x0, matrix products: 14.4 us -> none  [the longest x6 9.77 us: per_device(): jnp.dot(scaled, w, preferred_element_type=jnp.float32)]
    all_to_all x2 -> x0, starting transfers between devices: 8.84 us -> none  [the longest x1 4.48 us: per_device(): lax.all_to_all(attended, 'tp', split_axis=0, concat_axis=1, tiled=True)]
    all_to_all x2 -> x0, waiting for transfers between devices: 7.82 us -> none  [the longest x1 5.69 us: per_device(): lax.all_to_all(filtered, 'tp', split_axis=0, concat_axis=1, tiled=True)]
    unnamed x19 -> x3, local copies, waits for them, and re-layouts: 1.35 us -> 4.74 us
    reduce_sum x1 -> x0, other arithmetic: 3.22 us -> none  [per_device(): inverse = lax.rsqrt(jnp.mean(widened * widened, axis=1) + epsilon)]
    ppermute x1 -> x0, starting transfers between devices: 3.22 us -> none  [per_device(): lax.ppermute(product[n - rim:], 'sp', [(i, i + 1) for i in range(15)])]
  transfers between devices with their start and end apart: 4 -> 0, of which waited for: 3 -> 0; matrix products, arithmetic and copies ran while one was open for 6% -> 0% of each run, Pallas kernels for 48% -> 0%
where the time goes in v3:
time: 132 us; the launch traced here: 131 us
  Pallas kernels  126 us (95%)
  local copies, waits for them, and re-layouts  4.74 us (4%)
    pallas_call x1, Pallas kernels, per_device(): pl.pallas_call(layer_kernel, out_shape=(jax.ShapeDtypeStruct((128, 2048),...  126 us
    unnamed x3, local copies, waits for them, and re-layouts  4.74 us

profile of v3, /device:TPU:1, one launch (start us, length us, event | category | flops | bytes accessed | tf_op | source)
XLA Modules:
  0.0 131.3 jit_solution(1588564298333066056)
XLA Ops:
  0.6 1.6 %copy.14.bias = bf16[1024,2]{1,0:T(8,128)(2,1)} copy(bf16[1024,2]{0,1:T(2,128)(2,1)} %param.21) | data formatting | bytes 8192 | tf_op args[9]
  2.2 125.9 %shard_map.131 = (bf16[128,2048]{1,0:T(8,128)(2,1)}, f32[2,1024]{1,0:T(2,128)}) custom-call(bf16[1024,256]{1,0:T(8,128)(2,1)} %tokens.1, f32[1,2048]{1,0:T(1,128)} %bitcast.1, bf16[2048,128]{1,0:T(8,128)(2,1)} %w0.1, bf16[2048,128]{1,0:T(8,128)(2,1)} %w1.1, bf16[2048,128]{1,0:T(8,128)(2,1)} %w2.1, bf16[2048,128]{1,0:T(8,128)(2,1)} %w3.1, ...), custom_call_target="tpu_custom_call" | custom-call | tf_op jit(solution)/shard_map/pallas_call | solution.py:499
  128.1 1.9 %copy.17 = bf16[128,2048]{1,0:T(8,128)(2,1)} copy(bf16[128,2048]{1,0:T(8,128)(2,1)} %get-tuple-element.4) | data formatting | bytes 1048576
  130.0 1.3 copy.18

commit v4 on v3

--- a/solution.py
+++ b/solution.py
@@ -116,10 +116,10 @@
 
 
 def layer_kernel(tokens, gain, w0, w1, w2, w3, w4, w5, taps, bias, fr_hbm, ar_hbm, mixed, mass,
-                 tk, wts, fr, ar, sc, pr, post, fl, q, kp, vt, kb, vb, qb, rb, fa, at, total,
+                 tk, wts, fr, ar, sc, pr, post, fl, q, kvp, kvb, qb, rb, fa, at, total,
                  qt, out_local, carry_out, sums, carry, ya, yb, wa, wb,
                  lw, st, rt, sf, rim,
-                 rk, rv, rq, ro, rr, sk, sv, sq, so, sr, xk, xv, dk, dv, fk, sx, rx):
+                 rk, rq, ro, rr, sk, sq, so, sr, xk, dk, fk):
     me = lax.axis_index(SP)
     t = lax.axis_index(TP)
     z, x = me // 4, me % 4
@@ -130,6 +130,38 @@
     right = z * 4 + (x + 1) % 4
     left = z * 4 + (x + 3) % 4
 
+    back = t - core + z // 2
+    col, qcore, slot = query_place(z, x)
+    qtp = t - core + qcore
+
+    def query_local(l):
+        return (2 * core + l == z) & (col == x) & (qcore == core)
+
+    barrier = pltpu.get_barrier_semaphore()
+
+    def greet(sp, tp):
+        pl.semaphore_signal(barrier, inc=1, device_id={SP: sp, TP: tp}, device_id_type=pl.DeviceIdType.MESH)
+
+    for n in range(1, 8):
+        greet(me, (t + n) % 8)
+    greet(right, t)
+    greet(left, t)
+    for n in range(1, 4):
+        greet((me + 4 * n) % 16, t)
+    expected = 12
+    for s in range(2):
+        blk = set_block(x, core, s)
+
+        @pl.when(jnp.logical_not((blk == me) & (core == z // 2)))
+        def _():
+            greet(blk, back)
+        expected = expected + jnp.where(query_local(s), 0, 1)
+
+    @pl.when(me > 0)
+    def _():
+        greet(me - 1, t)
+    expected = expected + jnp.where(me < 15, 1, 0)
+
     local = [pltpu.make_async_copy(w, wts.at[:, i * 128:(i + 1) * 128], lw.at[i])
              for i, w in enumerate((w0, w1, w2, w3, w4, w5))]
     local += [pltpu.make_async_copy(fr_hbm, fr, lw.at[6]), pltpu.make_async_copy(ar_hbm, ar, lw.at[7])]
@@ -203,7 +235,7 @@
         pr[8 + k * CH:8 + (k + 1) * CH, :] = pre_gate.astype(jnp.float32) * signal.astype(jnp.float32)
         post[r, :] = post_gate
         q[:, r] = queries.astype(jnp.float32).T.astype(jnp.bfloat16)
-        b = bias[r, :].astype(jnp.float32) * LOG2E
+        b = jnp.concatenate([bias[:, r].astype(jnp.float32) * LOG2E, jnp.zeros((6, CH), jnp.float32)], axis=0).T
         wide = []
         for l in range(2):
             bl = b[:, l:l + 1]
@@ -214,63 +246,114 @@
             extra = jnp.where(lane == 64, hi, jnp.where(lane == 65, bl - hi, 0.0))
             wide.append(jnp.where(lane < 64, kf, extra).astype(jnp.bfloat16))
         kk = jnp.dot(order, jnp.concatenate(wide, axis=1), preferred_element_type=jnp.float32).astype(jnp.bfloat16)
-        kp[0, r, :] = kk[:, :128]
-        kp[1, r, :] = kk[:, 128:]
         vv = jnp.dot(order, values, preferred_element_type=jnp.float32).T.astype(jnp.bfloat16)
-        vt[0, k] = vv[:64]
-        vt[1, k] = vv[64:]
-
+        for l in range(2):
+            kvp[l, k, 0:256, :] = kk[:, l * 128:(l + 1) * 128]
+            kvp[l, k, 256:320, :] = vv[l * 64:(l + 1) * 64, :128]
+            kvp[l, k, 320:384, :] = vv[l * 64:(l + 1) * 64, 128:]
+
+    for c in local:
+        c.start()
+    tk[t] = tokens[...]
+    pl.semaphore_wait(barrier, expected)
     for k in range(2):
         for c in feature_sends(k):
             c.start()
-    for c in local:
-        c.start()
-    tk[t] = tokens[...]
+
+    def key_copy(l, k):
+        g = 2 * core + l
+        return remote(kvp.at[l, k], kvb.at[me, k], sk.at[l, k], rk.at[me, k], g * 4 + x, t)
+
+    def send_keys(k):
+        for l in range(2):
+            @pl.when(2 * core + l != z)
+            def _():
+                key_copy(l, k).start()
+
+            @pl.when(2 * core + l == z)
+            def _():
+                kvb[me, k] = kvp[l, k]
+
+    def pass_on(b, k, to, sem, tp=t, src=None):
+        return remote(kvb.at[b, k] if src is None else src, kvb.at[b, k], sem, rk.at[b, k], to, tp)
+
+    def arrived(b, k):
+        pass_on(b, k, me, sk.at[0, 0]).wait_recv()
+
+    def own_column(k):
+        @pl.when(active)
+        def _():
+            for zs in range(4):
+                b = zs * 4 + x
+
+                def spread(src):
+                    pass_on(b, k, right, xk.at[zs, k, 0], src=src).start()
+                    pass_on(b, k, left, xk.at[zs, k, 1], src=src).start()
+                    pass_on(b, k, me, dk.at[b, k], partner, src=src).start()
+
+                @pl.when(z != zs)
+                def _():
+                    arrived(b, k)
+                    spread(None)
+
+                @pl.when(z == zs)
+                def _():
+                    spread(kvp.at[zs % 2, k])
+
+    def near_columns(k):
+        @pl.when(active)
+        def _():
+            for zs in range(4):
+                even = (zs + k) % 2 == 0
+                b = zs * 4 + (x + 3) % 4
+                arrived(b, k)
+                if even:
+                    pass_on(b, k, right, fk.at[zs, k]).start()
+                pass_on(b, k, me, dk.at[b, k], partner).start()
+                b = zs * 4 + (x + 1) % 4
+                arrived(b, k)
+                if not even:
+                    pass_on(b, k, left, fk.at[zs, k]).start()
+                pass_on(b, k, me, dk.at[b, k], partner).start()
+
+    def far_column(k):
+        @pl.when(active)
+        def _():
+            for zs in range(4):
+                b = zs * 4 + (x + 2) % 4
+                arrived(b, k)
+                pass_on(b, k, me, dk.at[b, k], partner).start()
+
     near(0)
     near(1)
     rest(0)
     for c in local[:6]:
         c.wait()
     project(0)
+    send_keys(0)
     near(2)
     rest(1)
     project(1)
+    send_keys(1)
+    own_column(0)
     near(3)
     rest(2)
     project(2)
+    send_keys(2)
+    own_column(1)
+    near_columns(0)
     rest(3)
     project(3)
-
-    col, qcore, slot = query_place(z, x)
-    qtp = t - core + qcore
-
-    def key_copy(l):
-        g = 2 * core + l
-        return (remote(kp.at[l], kb.at[me], sk.at[l], rk.at[me], g * 4 + x, t),
-                remote(vt.at[l], vb.at[me], sv.at[l], rv.at[me], g * 4 + x, t))
+    send_keys(3)
 
     def query_copy(l):
         g = 2 * core + l
         return remote(q.at[pl.ds(l * 64, 64)], qb.at[slot], sq.at[l], rq.at[slot], g * 4 + col, qtp)
 
-    def query_local(l):
-        g = 2 * core + l
-        return (g == z) & (col == x) & (qcore == core)
-
     for l in range(2):
-        @pl.when(2 * core + l != z)
-        def _():
-            for c in key_copy(l):
-                c.start()
-
         @pl.when(jnp.logical_not(query_local(l)))
         def _():
             query_copy(l).start()
-
-        @pl.when(2 * core + l == z)
-        def _():
-            kb[me] = kp[l]
-            vb[me] = vt[l]
 
         @pl.when(query_local(l))
         def _():
@@ -283,41 +366,13 @@
     def _():
         rim_copy().start()
 
-    def pass_on(b, to, ks, vs, keys=True, values=True, tp=t, src=None):
-        ksrc, vsrc = src or (kb.at[b], vb.at[b])
-        if keys:
-            remote(ksrc, kb.at[b], ks, rk.at[b], to, tp).start()
-        if values:
-            remote(vsrc, vb.at[b], vs, rv.at[b], to, tp).start()
-
-    def sent(b, to, ks, vs, keys=True, values=True, tp=t):
-        if keys:
-            remote(kb.at[b], kb.at[b], ks, rk.at[b], to, tp).wait_send()
-        if values:
-            remote(vb.at[b], vb.at[b], vs, rv.at[b], to, tp).wait_send()
-
-    def arrived(b):
-        remote(kb.at[b], kb.at[b], sk.at[0], rk.at[b], me, t).wait_recv()
-        remote(vb.at[b], vb.at[b], sv.at[0], rv.at[b], me, t).wait_recv()
-
-    @pl.when(active)
-    def _():
-        for zs in (3, 2, 1, 0):
-            b = zs * 4 + x
-
-            def spread(src):
-                pass_on(b, right, xk.at[zs, 0], xv.at[zs, 0], src=src)
-                pass_on(b, left, xk.at[zs, 1], xv.at[zs, 1], src=src)
-                pass_on(b, me, dk.at[b], dv.at[b], tp=partner, src=src)
-
-            @pl.when(z != zs)
-            def _():
-                arrived(b)
-                spread(None)
-
-            @pl.when(z == zs)
-            def _():
-                spread((kp.at[zs % 2], vt.at[zs % 2]))
+    own_column(2)
+    near_columns(1)
+    far_column(0)
+
+    own_column(3)
+    near_columns(2)
+    far_column(1)
 
     @pl.when(me == 0)
     def _():
@@ -347,35 +402,22 @@
         filter_copy(n).start()
     fa[:, lanes(t)] = fl[lanes(t), :]
 
-    @pl.when(active)
-    def _():
-        for zs in (3, 2, 1, 0):
-            even = zs % 2 == 0
-            b = zs * 4 + (x + 3) % 4
-            arrived(b)
-            pass_on(b, right, fk.at[zs, 0], fk.at[zs, 0], keys=even, values=not even)
-            pass_on(b, me, dk.at[b], dv.at[b], tp=partner)
-            b = zs * 4 + (x + 1) % 4
-            arrived(b)
-            pass_on(b, left, fk.at[zs, 1], fk.at[zs, 1], keys=not even, values=even)
-            pass_on(b, me, dk.at[b], dv.at[b], tp=partner)
-        for zs in (3, 2, 1, 0):
-            b = zs * 4 + (x + 2) % 4
-            arrived(b)
-            pass_on(b, me, dk.at[b], dv.at[b], tp=partner)
+    near_columns(3)
+    far_column(2)
+    far_column(3)
 
     @pl.when(jnp.logical_not(active))
     def _():
         for b in range(16):
-            arrived(b)
+            for k in range(NT):
+                arrived(b, k)
 
     def kchunk(c):
-        return kb[c // NT, pl.ds(pl.multiple_of((c % NT) * CH, CH), CH), :]
+        return kvb[c // NT, c % NT, 0:256, :]
 
     def vchunk(c):
-        return vb[c // NT, c % NT]
-
-    back = t - core + z // 2
+        return jnp.concatenate([kvb[c // NT, c % NT, 256:320, :], kvb[c // NT, c % NT, 320:384, :]], axis=1)
+
     head_rows = pl.ds(pl.multiple_of((4 * y + z) * 64, 64), 64)
 
     def piece_copy(s, blk, p):
@@ -421,13 +463,16 @@
         def _():
             rb[z % 2] = carry_out[s]
 
-    for n in range(1, 8):
-        remote(fl.at[lanes(0)], fa.at[:, lanes((t - n + 8) % 8)], sf.at[n], sf.at[8 + n], me, t).wait_recv()
-    local[6].wait()
-    local[7].wait()
-    for n in range(8):
-        c = slice(n * 256, (n + 1) * 256)
-        total[:, c] = jnp.dot(fa[...], fr[:, c], preferred_element_type=jnp.float32)
+        if s == 0:
+            for n in range(1, 8):
+                remote(fl.at[lanes(0)], fa.at[:, lanes((t - n + 8) % 8)], sf.at[n], sf.at[8 + n], me, t).wait_recv()
+            local[6].wait()
+            local[7].wait()
+            for n in range(8):
+                c = slice(n * 256, (n + 1) * 256)
+                total[:, c] = jnp.dot(fa[...], fr[:, c], preferred_element_type=jnp.float32)
+
+
     for h in range(16):
         hz = h % 4
         column, hcore, _ = query_place(z, x)
@@ -445,7 +490,7 @@
         @pl.when(jnp.logical_not(query_local(l)))
         def _():
             remote(rb.at[l], rb.at[l], sr.at[0], rr.at[l], me, t).wait_recv()
-        mass[l:l + 1, :] = jnp.log(jnp.maximum(1.0 - rb[l, 0:1, :], mass_floor))
+        mass[l:l + 1, :] = rb[l, 0:1, :]
 
     for k in range(NT):
         for c in feature_sends(k):
@@ -458,8 +503,8 @@
     for l in range(2):
         @pl.when(2 * core + l != z)
         def _():
-            for c in key_copy(l):
-                c.wait_send()
+            for k in range(NT):
+                key_copy(l, k).wait_send()
 
         @pl.when(jnp.logical_not(query_local(l)))
         def _():
@@ -467,15 +512,13 @@
 
     @pl.when(active)
     def _():
-        for zs in (3, 2, 1, 0):
-            even = zs % 2 == 0
-            b = zs * 4 + x
-            sent(b, right, xk.at[zs, 0], xv.at[zs, 0])
-            sent(b, left, xk.at[zs, 1], xv.at[zs, 1])
-            sent(zs * 4 + (x + 3) % 4, right, fk.at[zs, 0], fk.at[zs, 0], keys=even, values=not even)
-            sent(zs * 4 + (x + 1) % 4, left, fk.at[zs, 1], fk.at[zs, 1], keys=not even, values=even)
-        for b in range(16):
-            sent(b, me, dk.at[b], dv.at[b], tp=partner)
+        for k in range(NT):
+            for zs in range(4):
+                pass_on(zs * 4 + x, k, right, xk.at[zs, k, 0]).wait_send()
+                pass_on(zs * 4 + x, k, left, xk.at[zs, k, 1]).wait_send()
+                pass_on(zs * 4 + x, k, right, fk.at[zs, k]).wait_send()
+            for b in range(16):
+                pass_on(b, k, me, dk.at[b, k], partner).wait_send()
 
     for s in range(2):
         blk = set_block(x, core, s)
@@ -496,7 +539,7 @@
     hbm = pl.BlockSpec(memory_space=pl.ANY)
     dma = pltpu.SemaphoreType.DMA
     bf16, f32 = jnp.bfloat16, jnp.float32
-    return pl.pallas_call(
+    mixed, remain = pl.pallas_call(
         layer_kernel,
         out_shape=(jax.ShapeDtypeStruct((128, 2048), bf16), jax.ShapeDtypeStruct((2, ROWS), f32)),
         in_specs=[vmem, vmem] + [hbm] * 6 + [vmem, vmem, hbm, hbm],
@@ -511,10 +554,8 @@
             pltpu.VMEM((ROWS, 128), bf16),
             pltpu.VMEM((ROWS, 128), bf16),
             pltpu.VMEM((128, ROWS), bf16),
-            pltpu.VMEM((2, ROWS, 128), bf16),
-            pltpu.VMEM((2, NT, 64, CH), bf16),
-            pltpu.VMEM((16, ROWS, 128), bf16),
-            pltpu.VMEM((16, NT, 64, CH), bf16),
+            pltpu.VMEM((2, NT, 384, 128), bf16),
+            pltpu.VMEM((16, NT, 384, 128), bf16),
             pltpu.VMEM((2, 64, ROWS), bf16),
             pltpu.VMEM((2, 8, ROWS), f32),
             pltpu.VMEM((128, 1024), bf16),
@@ -530,13 +571,14 @@
             pltpu.VMEM((NT, CH, CH), bf16),
             pltpu.VMEM((NT, CH, CH), bf16),
             dma((8,)), dma((4, 8)), dma((8, 4)), dma((16,)), dma((2,)),
-            dma((16,)), dma((16,)), dma((2,)), dma((16,)), dma((2,)),
-            dma((2,)), dma((2,)), dma((2,)), dma((2, 8)), dma((2,)),
-            dma((4, 2)), dma((4, 2)), dma((16,)), dma((16,)), dma((4, 2)), dma((2,)), dma((2,)),
+            dma((16, 4)), dma((2,)), dma((16,)), dma((2,)),
+            dma((2, 4)), dma((2,)), dma((2, 8)), dma((2,)),
+            dma((4, 4, 2)), dma((16, 4)), dma((4, 4)),
         ],
-        compiler_params=pltpu.CompilerParams(vmem_limit_bytes=60 * 2**20, has_side_effects=True),
+        compiler_params=pltpu.CompilerParams(vmem_limit_bytes=60 * 2**20, has_side_effects=True, collective_id=0),
     )(tokens, norm_gain.reshape(1, -1), signal_proj, postgate_proj, pregate_proj, query_proj, key_proj,
-      value_proj, filter_taps, break_bias, filter_readout, attention_readout)
+      value_proj, filter_taps, break_bias.T, filter_readout, attention_readout)
+    return mixed, jnp.log(jnp.maximum(1.0 - remain, mass_floor))
 
 
 def solution(mesh):

time: 132 us -> 109 us (0.83)
  Pallas kernels: 126 us -> 105 us
  local copies, waits for them, and re-layouts: 4.74 us -> 1.88 us
    pallas_call x1, Pallas kernels: 126 us -> 105 us  [per_device(): pl.pallas_call(layer_kernel, out_shape=(jax.ShapeDtypeStruct((128, 2048),...]
    unnamed x3 -> x1, local copies, waits for them, and re-layouts: 4.74 us -> 1.88 us
where the time goes in v4:
time: 109 us
  Pallas kernels  105 us (96%)
  local copies, waits for them, and re-layouts  1.88 us (2%)
  other arithmetic  1.31 us (1%)
    pallas_call x1, Pallas kernels, per_device(): pl.pallas_call(layer_kernel, out_shape=(jax.ShapeDtypeStruct((128, 2048),...  105 us

profile of v4, /device:TPU:1, one launch (start us, length us, event | category | flops | bytes accessed | tf_op | source)
XLA Modules:
  0.0 109.1 jit_solution(7868060842060098769)
XLA Ops:
  0.6 105.3 %shard_map.131 = (bf16[128,2048]{1,0:T(8,128)(2,1)}, f32[2,1024]{1,0:T(2,128)}) custom-call(bf16[1024,256]{1,0:T(8,128)(2,1)} %tokens.1, f32[1,2048]{1,0:T(1,128)} %bitcast.2, bf16[2048,128]{1,0:T(8,128)(2,1)} %w0.1, bf16[2048,128]{1,0:T(8,128)(2,1)} %w1.1, bf16[2048,128]{1,0:T(8,128)(2,1)} %w2.1, bf16[2048,128]{1,0:T(8,128)(2,1)} %w3.1, ...), custom_call_target="tpu_custom_call" | custom-call | tf_op jit(solution)/shard_map/pallas_call | solution.py:542
  105.9 1.3 %maximum_log_fusion = f32[2,1024]{1,0:T(2,128)} fusion(f32[2,1024]{1,0:T(2,128)} %get-tuple-element.5), kind=kLoop, calls=%fused_computation | loop fusion | flops 4096 | bytes 16384 | tf_op jit(solution)/shard_map/log | solution.py:581
  107.3 1.9 %copy.15 = bf16[128,2048]{1,0:T(8,128)(2,1)} copy(bf16[128,2048]{1,0:T(8,128)(2,1)} %get-tuple-element.8) | data formatting | bytes 1048576

commit v5 on v4

--- a/solution.py
+++ b/solution.py
@@ -10,52 +10,51 @@
 CH = 256
 NT = 4
 CAP = 24.0
+QROWS = 256
 LOG2E = 1.4426950408889634
 epsilon = 1e-06
 mass_floor = 0.1
 
 
 def scan_chunk(y_ref, carry_ref, w_ref, masked):
-    groups = CH // 8
     seg = CH // 8
     if masked:
         row = lax.broadcasted_iota(jnp.int32, (8, CH), 0) * seg
         col = lax.broadcasted_iota(jnp.int32, (8, CH), 1)
         diff = col - row
     r = jnp.ones((8, CH), jnp.float32)
-    for g in reversed(range(groups // 4)):
+    for g in reversed(range(seg // 4)):
         us, ds = [], []
         for k in range(4):
             j = 4 * g + k
-            y = y_ref[j * 8:(j + 1) * 8, :]
-            u = jnp.exp2(jnp.minimum(y, CAP))
+            u = jnp.exp2(jnp.minimum(y_ref[j * 8:(j + 1) * 8, :], CAP))
             if masked:
                 u = jnp.where(diff > j, u, 0.0)
             us.append(u)
             ds.append(1.0 + u)
-        prod = (ds[0] * ds[1]) * (ds[2] * ds[3])
-        r = r * (1.0 / prod)
-        e = r
-        for k in range(4):
+        low, high = ds[0] * ds[1], ds[2] * ds[3]
+        r = r * (1.0 / (low * high))
+        e = r * low
+        ws = [us[0] * r, us[1] * (r * ds[0]), us[2] * e, us[3] * (e * ds[2])]
+        for k in (0, 2):
             j = 4 * g + k
-            y_ref[j * 8:(j + 1) * 8, :] = us[k] * e
-            if k < 3:
-                e = e * ds[k]
+            w_ref[j * 8:(j + 2) * 8, :] = jnp.concatenate(ws[k:k + 2], axis=0).astype(jnp.bfloat16)
     sub = lax.broadcasted_iota(jnp.int32, (8, CH), 0)
     s = r
     for k in (1, 2, 4):
         s = s * jnp.where(sub < 8 - k, pltpu.roll(s, 8 - k, 0), 1.0)
-    excl = jnp.where(sub < 7, pltpu.roll(s, 7, 0), 1.0)
     carry = carry_ref[...]
-    c = excl * carry
+    c = jnp.where(sub < 7, pltpu.roll(s, 7, 0), 1.0) * carry
     carry_ref[...] = carry * jnp.broadcast_to(s[0:1, :], (8, CH))
-    w = y_ref[...].reshape(CH // 8, 8, CH) * c[None]
-    w_ref[...] = w.reshape(CH, CH).astype(jnp.bfloat16)
-
-def qk(k_ref, q_ref, tile):
-    kk = k_ref
-    return jnp.dot(jnp.concatenate([kk, kk], axis=1), q_ref[:, tile * CH:(tile + 1) * CH],
-                   preferred_element_type=jnp.float32)
+    c = jnp.concatenate([c, c], axis=0).astype(jnp.bfloat16)
+    for j in range(CH // 16):
+        w_ref[j * 16:(j + 1) * 16, :] = w_ref[j * 16:(j + 1) * 16, :] * c
+
+def scores_to(y_ref, kk, q_ref, tile):
+    lhs = jnp.concatenate([kk, kk], axis=1)
+    rhs = q_ref[:, tile * CH:(tile + 1) * CH]
+    for i in range(0, CH, QROWS):
+        y_ref[i:i + QROWS, :] = jnp.dot(lhs[i:i + QROWS], rhs, preferred_element_type=jnp.float32)
 
 def attend_set(qt, blk, kchunk, vchunk, acc, carry, ya, yb, wa, wb):
     base = 4 * blk
@@ -65,7 +64,7 @@
     for c in reversed(range(NT)):
         kk = kchunk(base + c)
         for t in range(c, NT):
-            ya[t] = qk(kk, qt, t)
+            scores_to(ya.at[t], kk, qt, t)
         for t in range(c, NT):
             scan_chunk(ya.at[t], carry.at[t], wb.at[t], t == c)
         if c > 0:
@@ -74,14 +73,14 @@
                 acc[t] += jnp.dot(vv, wb[t], preferred_element_type=jnp.float32)
     kk = kchunk(jnp.maximum(base - 1, 0))
     for t in range(NT):
-        ya[t] = qk(kk, qt, t)
+        scores_to(ya.at[t], kk, qt, t)
 
     def half(c, ysrc, ydst, wdst, wsrc):
         kn = kchunk(jnp.maximum(c - 1, 0))
         vp = vchunk(c + 1)
         for t in range(NT):
             scan_chunk(ysrc.at[t], carry.at[t], wdst.at[t], False)
-            ydst[t] = qk(kn, qt, t)
+            scores_to(ydst.at[t], kn, qt, t)
             acc[t] += jnp.dot(vp, wsrc[t], preferred_element_type=jnp.float32)
 
     def body(p, _):
@@ -116,7 +115,7 @@
 
 
 def layer_kernel(tokens, gain, w0, w1, w2, w3, w4, w5, taps, bias, fr_hbm, ar_hbm, mixed, mass,
-                 tk, wts, fr, ar, sc, pr, post, fl, q, kvp, kvb, qb, rb, fa, at, total,
+                 tk, wts, fr, ar, sc, pr, post, fl, q, kvp, kvb, kx, qb, rb, fa, at, total,
                  qt, out_local, carry_out, sums, carry, ya, yb, wa, wb,
                  lw, st, rt, sf, rim,
                  rk, rq, ro, rr, sk, sq, so, sr, xk, dk, fk):
@@ -212,7 +211,7 @@
     rowi = lax.broadcasted_iota(jnp.int32, (CH, CH), 0)
     coli = lax.broadcasted_iota(jnp.int32, (CH, CH), 1)
     order = jnp.where(coli == (rowi % 8) * (CH // 8) + rowi // 8, 1.0, 0.0).astype(jnp.bfloat16)
-    lane = lax.broadcasted_iota(jnp.int32, (CH, 128), 1)
+    half = lax.broadcasted_iota(jnp.int32, (128, 128), 1) < 64
 
     def project(k):
         r = rows(k)
@@ -235,22 +234,21 @@
         pr[8 + k * CH:8 + (k + 1) * CH, :] = pre_gate.astype(jnp.float32) * signal.astype(jnp.float32)
         post[r, :] = post_gate
         q[:, r] = queries.astype(jnp.float32).T.astype(jnp.bfloat16)
-        b = jnp.concatenate([bias[:, r].astype(jnp.float32) * LOG2E, jnp.zeros((6, CH), jnp.float32)], axis=0).T
-        wide = []
-        for l in range(2):
-            bl = b[:, l:l + 1]
-            hi = bl.astype(jnp.bfloat16).astype(jnp.float32)
-            kf = keys.astype(jnp.float32)
-            if l == 1:
-                kf = pltpu.roll(kf, 64, 1)
-            extra = jnp.where(lane == 64, hi, jnp.where(lane == 65, bl - hi, 0.0))
-            wide.append(jnp.where(lane < 64, kf, extra).astype(jnp.bfloat16))
-        kk = jnp.dot(order, jnp.concatenate(wide, axis=1), preferred_element_type=jnp.float32).astype(jnp.bfloat16)
+        b = bias[:, r].astype(jnp.float32) * LOG2E
+        hi = b.astype(jnp.bfloat16).astype(jnp.float32)
+        four = jnp.concatenate([hi[0:1], (b - hi)[0:1], hi[1:2], (b - hi)[1:2], jnp.zeros((4, CH), jnp.float32)], axis=0)
+        four = lax.dot_general(four.astype(jnp.bfloat16), order, (((1,), (1,)), ((), ())),
+                               preferred_element_type=jnp.float32)
+        four = jnp.concatenate([four[:, :128], four[:, 128:]], axis=0).astype(jnp.bfloat16)
+        kk = jnp.dot(order, keys, preferred_element_type=jnp.float32)
+        top, bottom = kk[:128], kk[128:]
+        packed = (jnp.where(half, top, pltpu.roll(bottom, 64, 1)), jnp.where(half, pltpu.roll(top, 64, 1), bottom))
         vv = jnp.dot(order, values, preferred_element_type=jnp.float32).T.astype(jnp.bfloat16)
         for l in range(2):
-            kvp[l, k, 0:256, :] = kk[:, l * 128:(l + 1) * 128]
-            kvp[l, k, 256:320, :] = vv[l * 64:(l + 1) * 64, :128]
-            kvp[l, k, 320:384, :] = vv[l * 64:(l + 1) * 64, 128:]
+            kvp[l, k, 0:128, :] = packed[l].astype(jnp.bfloat16)
+            kvp[l, k, 128:192, :] = vv[l * 64:(l + 1) * 64, :128]
+            kvp[l, k, 192:256, :] = vv[l * 64:(l + 1) * 64, 128:]
+            kvp[l, k, 256:272, :] = four
 
     for c in local:
         c.start()
@@ -259,6 +257,7 @@
     for k in range(2):
         for c in feature_sends(k):
             c.start()
+
 
     def key_copy(l, k):
         g = 2 * core + l
@@ -323,6 +322,30 @@
                 b = zs * 4 + (x + 2) % 4
                 arrived(b, k)
                 pass_on(b, k, me, dk.at[b, k], partner).start()
+
+    brow = lax.broadcasted_iota(jnp.int32, (16, 256), 0)
+    bcol = lax.broadcasted_iota(jnp.int32, (16, 256), 1)
+    bpart = bcol % 128 - 64
+    select = jnp.where((bpart >= 0) & (bpart < 2) & (brow == (bcol // 128) * 8 + 2 * (z % 2) + bpart), 1.0, 0.0)
+    select = select.astype(jnp.bfloat16)
+
+    def unpack(k):
+        def four(n, _):
+            for i in range(4):
+                b = 4 * n + i
+                packed = kvb[b, k, 0:128, :].astype(jnp.float32)
+                extra = lax.dot_general(kvb[b, k, 256:272, :], select, (((0,), (0,)), ((), ())),
+                                        preferred_element_type=jnp.float32)
+                kx[b, k, 0:128, :] = jnp.where(half, packed, extra[:, :128]).astype(jnp.bfloat16)
+                kx[b, k, 128:256, :] = jnp.where(half, pltpu.roll(packed, 64, 1), extra[:, 128:]).astype(jnp.bfloat16)
+            return 0
+        lax.fori_loop(0, 4, four, 0)
+
+    def passive_arrivals(k):
+        @pl.when(jnp.logical_not(active))
+        def _():
+            for b in range(16):
+                arrived(b, k)
 
     near(0)
     near(1)
@@ -369,7 +392,6 @@
     own_column(2)
     near_columns(1)
     far_column(0)
-
     own_column(3)
     near_columns(2)
     far_column(1)
@@ -403,20 +425,22 @@
     fa[:, lanes(t)] = fl[lanes(t), :]
 
     near_columns(3)
+    passive_arrivals(0)
+    unpack(0)
+    passive_arrivals(1)
+    unpack(1)
     far_column(2)
+    passive_arrivals(2)
+    unpack(2)
     far_column(3)
-
-    @pl.when(jnp.logical_not(active))
-    def _():
-        for b in range(16):
-            for k in range(NT):
-                arrived(b, k)
+    passive_arrivals(3)
+    unpack(3)
 
     def kchunk(c):
-        return kvb[c // NT, c % NT, 0:256, :]
+        return kx[c // NT, c % NT]
 
     def vchunk(c):
-        return jnp.concatenate([kvb[c // NT, c % NT, 256:320, :], kvb[c // NT, c % NT, 320:384, :]], axis=1)
+        return jnp.concatenate([kvb[c // NT, c % NT, 128:192, :], kvb[c // NT, c % NT, 192:256, :]], axis=1)
 
     head_rows = pl.ds(pl.multiple_of((4 * y + z) * 64, 64), 64)
 
@@ -554,8 +578,9 @@
             pltpu.VMEM((ROWS, 128), bf16),
             pltpu.VMEM((ROWS, 128), bf16),
             pltpu.VMEM((128, ROWS), bf16),
-            pltpu.VMEM((2, NT, 384, 128), bf16),
-            pltpu.VMEM((16, NT, 384, 128), bf16),
+            pltpu.VMEM((2, NT, 272, 128), bf16),
+            pltpu.VMEM((16, NT, 272, 128), bf16),
+            pltpu.VMEM((16, NT, CH, 128), bf16),
             pltpu.VMEM((2, 64, ROWS), bf16),
             pltpu.VMEM((2, 8, ROWS), f32),
             pltpu.VMEM((128, 1024), bf16),

time: 109 us -> 103 us (0.945)
  Pallas kernels: 105 us -> 99.3 us
    pallas_call x1, Pallas kernels: 105 us -> 99.3 us  [per_device(): pl.pallas_call(layer_kernel, out_shape=(jax.ShapeDtypeStruct((128, 2048),...]
where the time goes in v5:
time: 103 us
  Pallas kernels  99.3 us (96%)
  local copies, waits for them, and re-layouts  1.88 us (2%)
  other arithmetic  1.31 us (1%)
    pallas_call x1, Pallas kernels, per_device(): pl.pallas_call(layer_kernel, out_shape=(jax.ShapeDtypeStruct((128, 2048),...  99.3 us

profile of v5, /device:TPU:1, one launch (start us, length us, event | category | flops | bytes accessed | tf_op | source)
XLA Modules:
  0.0 103.1 jit_solution(6081855743161432755)
XLA Ops:
  0.6 99.3 %shard_map.131 = (bf16[128,2048]{1,0:T(8,128)(2,1)}, f32[2,1024]{1,0:T(2,128)}) custom-call(bf16[1024,256]{1,0:T(8,128)(2,1)} %tokens.1, f32[1,2048]{1,0:T(1,128)} %bitcast.2, bf16[2048,128]{1,0:T(8,128)(2,1)} %w0.1, bf16[2048,128]{1,0:T(8,128)(2,1)} %w1.1, bf16[2048,128]{1,0:T(8,128)(2,1)} %w2.1, bf16[2048,128]{1,0:T(8,128)(2,1)} %w3.1, ...), custom_call_target="tpu_custom_call" | custom-call | tf_op jit(solution)/shard_map/pallas_call | solution.py:566
  99.9 1.3 %maximum_log_fusion = f32[2,1024]{1,0:T(2,128)} fusion(f32[2,1024]{1,0:T(2,128)} %get-tuple-element.5), kind=kLoop, calls=%fused_computation | loop fusion | flops 4096 | bytes 16384 | tf_op jit(solution)/shard_map/log | solution.py:606
  101.2 1.9 %copy.15 = bf16[128,2048]{1,0:T(8,128)(2,1)} copy(bf16[128,2048]{1,0:T(8,128)(2,1)} %get-tuple-element.8) | data formatting | bytes 1048576

commit v6 on v5

--- a/solution.py
+++ b/solution.py
@@ -56,7 +56,7 @@
     for i in range(0, CH, QROWS):
         y_ref[i:i + QROWS, :] = jnp.dot(lhs[i:i + QROWS], rhs, preferred_element_type=jnp.float32)
 
-def attend_set(qt, blk, kchunk, vchunk, acc, carry, ya, yb, wa, wb):
+def attend_own(qt, blk, kchunk, vchunk, acc, carry, ya, wb):
     base = 4 * blk
     for t in range(NT):
         acc[t] = jnp.zeros_like(acc[t])
@@ -71,6 +71,10 @@
             vv = vchunk(base + c)
             for t in range(c, NT):
                 acc[t] += jnp.dot(vv, wb[t], preferred_element_type=jnp.float32)
+
+
+def attend_before(qt, blk, kchunk, vchunk, acc, carry, ya, yb, wa, wb):
+    base = 4 * blk
     kk = kchunk(jnp.maximum(base - 1, 0))
     for t in range(NT):
         scores_to(ya.at[t], kk, qt, t)
@@ -329,23 +333,24 @@
     select = jnp.where((bpart >= 0) & (bpart < 2) & (brow == (bcol // 128) * 8 + 2 * (z % 2) + bpart), 1.0, 0.0)
     select = select.astype(jnp.bfloat16)
 
-    def unpack(k):
-        def four(n, _):
-            for i in range(4):
-                b = 4 * n + i
+    def unpack(column):
+        def chunk(k, _):
+            for zs in range(4):
+                b = zs * 4 + column
                 packed = kvb[b, k, 0:128, :].astype(jnp.float32)
                 extra = lax.dot_general(kvb[b, k, 256:272, :], select, (((0,), (0,)), ((), ())),
                                         preferred_element_type=jnp.float32)
                 kx[b, k, 0:128, :] = jnp.where(half, packed, extra[:, :128]).astype(jnp.bfloat16)
                 kx[b, k, 128:256, :] = jnp.where(half, pltpu.roll(packed, 64, 1), extra[:, 128:]).astype(jnp.bfloat16)
             return 0
-        lax.fori_loop(0, 4, four, 0)
-
-    def passive_arrivals(k):
+        lax.fori_loop(0, NT, chunk, 0)
+
+    def passive_arrivals(column):
         @pl.when(jnp.logical_not(active))
         def _():
-            for b in range(16):
-                arrived(b, k)
+            for k in range(NT):
+                for zs in range(4):
+                    arrived(zs * 4 + column, k)
 
     near(0)
     near(1)
@@ -374,10 +379,6 @@
         return remote(q.at[pl.ds(l * 64, 64)], qb.at[slot], sq.at[l], rq.at[slot], g * 4 + col, qtp)
 
     for l in range(2):
-        @pl.when(jnp.logical_not(query_local(l)))
-        def _():
-            query_copy(l).start()
-
         @pl.when(query_local(l))
         def _():
             qb[slot] = q[l * 64:(l + 1) * 64, :]
@@ -394,8 +395,43 @@
     far_column(0)
     own_column(3)
     near_columns(2)
+    for l in range(2):
+        @pl.when(jnp.logical_not(query_local(l)))
+        def _():
+            query_copy(l).start()
     far_column(1)
 
+
+    def kchunk(c):
+        return kx[c // NT, c % NT]
+
+    def vchunk(c):
+        return jnp.concatenate([kvb[c // NT, c % NT, 128:192, :], kvb[c // NT, c % NT, 192:256, :]], axis=1)
+
+    head_rows = pl.ds(pl.multiple_of((4 * y + z) * 64, 64), 64)
+
+    def piece_copy(s, blk, p):
+        return remote(out_local.at[s, :, pl.ds(p * 128, 128)], at.at[head_rows], so.at[s, p],
+                      ro.at[4 * y + z], blk, p)
+
+    def rem_copy(s, blk):
+        return remote(carry_out.at[s], rb.at[z % 2], sr.at[s], rr.at[z % 2], blk, back)
+
+    def first_part(s):
+        blk = set_block(x, core, s)
+
+        @pl.when(jnp.logical_not((blk == me) & (core == z // 2)))
+        def _():
+            remote(qb.at[s], qb.at[s], sq.at[0], rq.at[s], me, t).wait_recv()
+        qs = qb[s].astype(jnp.float32) * (HEAD_DIM ** -0.5 * LOG2E)
+        hi = qs.astype(jnp.bfloat16)
+        qt[s, 0:64] = hi
+        qt[s, 64:128] = jnp.where(lax.broadcasted_iota(jnp.int32, (64, ROWS), 0) < 2, 1.0, 0.0).astype(jnp.bfloat16)
+        qt[s, 128:192] = (qs - hi.astype(jnp.float32)).astype(jnp.bfloat16)
+        qt[s, 192:256] = jnp.zeros((64, ROWS), jnp.bfloat16)
+        attend_own(qt.at[s], blk, kchunk, vchunk, sums.at[s], carry.at[s], ya, wb.at[s])
+
+    near_columns(3)
     @pl.when(me == 0)
     def _():
         pr[0:8, :] = jnp.zeros((8, 128), jnp.float32)
@@ -423,51 +459,23 @@
     for n in range(1, 8):
         filter_copy(n).start()
     fa[:, lanes(t)] = fl[lanes(t), :]
-
-    near_columns(3)
-    passive_arrivals(0)
-    unpack(0)
-    passive_arrivals(1)
-    unpack(1)
+    for c in (0, 3, 1):
+        passive_arrivals((x + c) % 4)
+        unpack((x + c) % 4)
     far_column(2)
-    passive_arrivals(2)
-    unpack(2)
+    first_part(1)
     far_column(3)
-    passive_arrivals(3)
-    unpack(3)
-
-    def kchunk(c):
-        return kx[c // NT, c % NT]
-
-    def vchunk(c):
-        return jnp.concatenate([kvb[c // NT, c % NT, 128:192, :], kvb[c // NT, c % NT, 192:256, :]], axis=1)
-
-    head_rows = pl.ds(pl.multiple_of((4 * y + z) * 64, 64), 64)
-
-    def piece_copy(s, blk, p):
-        return remote(out_local.at[s, :, pl.ds(p * 128, 128)], at.at[head_rows], so.at[s, p],
-                      ro.at[4 * y + z], blk, p)
-
-    def rem_copy(s, blk):
-        return remote(carry_out.at[s], rb.at[z % 2], sr.at[s], rr.at[z % 2], blk, back)
+    first_part(0)
+    passive_arrivals((x + 2) % 4)
+    unpack((x + 2) % 4)
 
     for s in range(2):
         blk = set_block(x, core, s)
         own = (blk == me) & (core == z // 2)
-
-        @pl.when(jnp.logical_not(own))
-        def _():
-            remote(qb.at[s], qb.at[s], sq.at[0], rq.at[s], me, t).wait_recv()
-        qs = qb[s].astype(jnp.float32) * (HEAD_DIM ** -0.5 * LOG2E)
-        hi = qs.astype(jnp.bfloat16)
-        qt[0:64] = hi
-        qt[64:128] = jnp.where(lax.broadcasted_iota(jnp.int32, (64, ROWS), 0) < 2, 1.0, 0.0).astype(jnp.bfloat16)
-        qt[128:192] = (qs - hi.astype(jnp.float32)).astype(jnp.bfloat16)
-        qt[192:256] = jnp.zeros((64, ROWS), jnp.bfloat16)
-        attend_set(qt, blk, kchunk, vchunk, sums, carry, ya, yb, wa, wb)
+        attend_before(qt.at[s], blk, kchunk, vchunk, sums.at[s], carry.at[s], ya, yb, wa, wb.at[s])
         for i in range(NT):
-            out_local[s, :, i * CH:(i + 1) * CH] = sums[i].astype(jnp.bfloat16)
-            carry_out[s, :, i * CH:(i + 1) * CH] = carry[i]
+            out_local[s, :, i * CH:(i + 1) * CH] = sums[s, i].astype(jnp.bfloat16)
+            carry_out[s, :, i * CH:(i + 1) * CH] = carry[s, i]
         for p in range(8):
             here = (blk == me) & (t == p)
 
@@ -586,15 +594,15 @@
             pltpu.VMEM((128, 1024), bf16),
             pltpu.VMEM((1024, 128), bf16),
             pltpu.VMEM((128, 2048), f32),
-            pltpu.VMEM((256, ROWS), bf16),
+            pltpu.VMEM((2, 256, ROWS), bf16),
             pltpu.VMEM((2, 64, ROWS), bf16),
             pltpu.VMEM((2, 8, ROWS), f32),
-            pltpu.VMEM((NT, 64, CH), f32),
-            pltpu.VMEM((NT, 8, CH), f32),
+            pltpu.VMEM((2, NT, 64, CH), f32),
+            pltpu.VMEM((2, NT, 8, CH), f32),
             pltpu.VMEM((NT, CH, CH), f32),
             pltpu.VMEM((NT, CH, CH), f32),
             pltpu.VMEM((NT, CH, CH), bf16),
-            pltpu.VMEM((NT, CH, CH), bf16),
+            pltpu.VMEM((2, NT, CH, CH), bf16),
             dma((8,)), dma((4, 8)), dma((8, 4)), dma((16,)), dma((2,)),
             dma((16, 4)), dma((2,)), dma((16,)), dma((2,)),
             dma((2, 4)), dma((2,)), dma((2, 8)), dma((2,)),

time: 103 us -> 100 us (0.971)
  Pallas kernels: 99.3 us -> 96.3 us
    pallas_call x1, Pallas kernels: 99.3 us -> 96.3 us  [per_device(): pl.pallas_call(layer_kernel, out_shape=(jax.ShapeDtypeStruct((128, 2048),...]
where the time goes in v6:
time: 100 us
  Pallas kernels  96.3 us (96%)
  local copies, waits for them, and re-layouts  1.88 us (2%)
  other arithmetic  1.31 us (1%)
    pallas_call x1, Pallas kernels, per_device(): pl.pallas_call(layer_kernel, out_shape=(jax.ShapeDtypeStruct((128, 2048),...  96.3 us

profile of v6, /device:TPU:1, one launch (start us, length us, event | category | flops | bytes accessed | tf_op | source)
XLA Modules:
  0.0 100.1 jit_solution(17327625344257027671)
XLA Ops:
  0.6 96.3 %shard_map.131 = (bf16[128,2048]{1,0:T(8,128)(2,1)}, f32[2,1024]{1,0:T(2,128)}) custom-call(bf16[1024,256]{1,0:T(8,128)(2,1)} %tokens.1, f32[1,2048]{1,0:T(1,128)} %bitcast.2, bf16[2048,128]{1,0:T(8,128)(2,1)} %w0.1, bf16[2048,128]{1,0:T(8,128)(2,1)} %w1.1, bf16[2048,128]{1,0:T(8,128)(2,1)} %w2.1, bf16[2048,128]{1,0:T(8,128)(2,1)} %w3.1, ...), custom_call_target="tpu_custom_call" | custom-call | tf_op jit(solution)/shard_map/pallas_call | solution.py:574
  96.9 1.3 %maximum_log_fusion = f32[2,1024]{1,0:T(2,128)} fusion(f32[2,1024]{1,0:T(2,128)} %get-tuple-element.5), kind=kLoop, calls=%fused_computation | loop fusion | flops 4096 | bytes 16384 | tf_op jit(solution)/shard_map/log | solution.py:614
  98.2 1.9 %copy.15 = bf16[128,2048]{1,0:T(8,128)(2,1)} copy(bf16[128,2048]{1,0:T(8,128)(2,1)} %get-tuple-element.8) | data formatting | bytes 1048576

commit v7 on v6

--- a/solution.py
+++ b/solution.py
@@ -410,8 +410,9 @@
 
     head_rows = pl.ds(pl.multiple_of((4 * y + z) * 64, 64), 64)
 
-    def piece_copy(s, blk, p):
-        return remote(out_local.at[s, :, pl.ds(p * 128, 128)], at.at[head_rows], so.at[s, p],
+    def piece_copy(s, blk, n):
+        p = (t + n) % 8
+        return remote(out_local.at[s, :, lanes(p)], at.at[head_rows], so.at[s, n],
                       ro.at[4 * y + z], blk, p)
 
     def rem_copy(s, blk):
@@ -477,7 +478,7 @@
             out_local[s, :, i * CH:(i + 1) * CH] = sums[s, i].astype(jnp.bfloat16)
             carry_out[s, :, i * CH:(i + 1) * CH] = carry[s, i]
         for p in range(8):
-            here = (blk == me) & (t == p)
+            here = (blk == me) & (p == 0)
 
             @pl.when(jnp.logical_not(here))
             def _():
@@ -485,7 +486,7 @@
 
             @pl.when(here)
             def _():
-                at[head_rows, :] = out_local[s, :, p * 128:(p + 1) * 128]
+                at[head_rows, :] = out_local[s, :, lanes((t + p) % 8)]
 
         @pl.when(jnp.logical_not(own))
         def _():
@@ -556,7 +557,7 @@
         blk = set_block(x, core, s)
         own = (blk == me) & (core == z // 2)
         for p in range(8):
-            @pl.when(jnp.logical_not((blk == me) & (t == p)))
+            @pl.when(jnp.logical_not((blk == me) & (p == 0)))
             def _():
                 piece_copy(s, blk, p).wait_send()
 

time: 100 us -> 100 us (level)
  no operation moved by 1% of the time
where the time goes in v7:
time: 100 us
  Pallas kernels  96.3 us (96%)
  local copies, waits for them, and re-layouts  1.88 us (2%)
  other arithmetic  1.31 us (1%)
    pallas_call x1, Pallas kernels, per_device(): pl.pallas_call(layer_kernel, out_shape=(jax.ShapeDtypeStruct((128, 2048),...  96.3 us

profile of v7, /device:TPU:1, one launch (start us, length us, event | category | flops | bytes accessed | tf_op | source)
XLA Modules:
  0.0 100.1 jit_solution(573885181628735555)
XLA Ops:
  0.6 96.3 %shard_map.131 = (bf16[128,2048]{1,0:T(8,128)(2,1)}, f32[2,1024]{1,0:T(2,128)}) custom-call(bf16[1024,256]{1,0:T(8,128)(2,1)} %tokens.1, f32[1,2048]{1,0:T(1,128)} %bitcast.2, bf16[2048,128]{1,0:T(8,128)(2,1)} %w0.1, bf16[2048,128]{1,0:T(8,128)(2,1)} %w1.1, bf16[2048,128]{1,0:T(8,128)(2,1)} %w2.1, bf16[2048,128]{1,0:T(8,128)(2,1)} %w3.1, ...), custom_call_target="tpu_custom_call" | custom-call | tf_op jit(solution)/shard_map/pallas_call | solution.py:575
  96.9 1.3 %maximum_log_fusion = f32[2,1024]{1,0:T(2,128)} fusion(f32[2,1024]{1,0:T(2,128)} %get-tuple-element.5), kind=kLoop, calls=%fused_computation | loop fusion | flops 4096 | bytes 16384 | tf_op jit(solution)/shard_map/log | solution.py:615
  98.2 1.9 %copy.15 = bf16[128,2048]{1,0:T(8,128)(2,1)} copy(bf16[128,2048]{1,0:T(8,128)(2,1)} %get-tuple-element.8) | data formatting | bytes 1048576
